TPU v7x, 32 devices: a whole 2x2x4 slice. The times are simulated.
32 devices in a mesh: sp: 8 (over z, y), tp: 4 (over x, core).
Axes of the slice: x: 2, y: 2, z: 4, core: 2. Of those that a mesh axis runs over, the one named last changes fastest.
Arguments:
- tokens: bfloat16 [1024, 2048], P(('sp', 'tp')), may hold values from -8.5 to 8.5
- norm_gain: bfloat16 [2048], replicated, may hold values from 0.099609375 to 1.8984375
- w_query: bfloat16 [2048, 1024], P(None, 'tp'), may hold values from -0.088388348 to 0.088388348
- w_key: bfloat16 [2048, 512], P(None, 'tp'), may hold values from -5.3298174 to 5.3298174
- w_value: bfloat16 [2048, 512], P(None, 'tp'), may hold values from -0.125 to 0.125
- w_conv_value: bfloat16 [2048, 1024], P(None, 'tp'), may hold values from -0.125 to 0.125
- w_conv_gate: bfloat16 [2048, 1024], P(None, 'tp'), may hold values from -0.125 to 0.125
- conv_taps: bfloat16 [31, 1024], P(None, 'tp'), may hold values from -1 to 1
- conv_gain: bfloat16 [1024], P('tp'), may hold values from 0.099609375 to 1.8984375
- conv_bias: bfloat16 [1024], P('tp'), may hold values from -3 to 3
- cum_gate: float32 [1024, 8], P(None, 'tp'), may hold values from -125 to 0, as said below
- w_out_att: bfloat16 [1024, 2048], P('tp', 'sp'), may hold values from -0.28125 to 0.28125
- w_out_conv: bfloat16 [1024, 2048], P('tp', 'sp'), may hold values from -0.1875 to 0.1875
Outputs:
- mixed_out: bfloat16 [1024, 2048], P('sp', 'tp')
Inputs may be any that keep to these rules, and one draw needn't show every extreme that they name: `cum_gate`: in each head, non-increasing along positions, and at most 0.
All inputs are finite; a program needn't handle non-finite values.
Results may differ from a plain program's by a relative error of at most 0.012.
Values may be sent and summed in bfloat16 or wider, within the bound.
A program may use at most 64 MiB of HBM per device.

v0:
```python
import functools
import math

import jax
import jax.numpy as jnp
from jax import lax
from jax.experimental import pallas as pl
from jax.experimental.pallas import tpu as pltpu
from jax.sharding import PartitionSpec as P

HEAD = 128
CONV = 1024
KW = 31


def shifted(array, axis, by):
    peers = lax.axis_size(axis)
    pairs = [(i, i + by) for i in range(peers) if 0 <= i + by < peers]
    return lax.ppermute(array, axis, pairs)


def shards(
    tokens,
    norm_gain,
    w_query,
    w_key,
    w_value,
    w_conv_value,
    w_conv_gate,
    conv_taps,
    conv_gain,
    conv_bias,
    cum_gate,
    w_out_att,
    w_out_conv,
):
    query_cols = w_query.shape[1]
    kv_cols = w_key.shape[1]
    conv_cols = w_conv_value.shape[1]
    head_count = query_cols // HEAD
    kv_count = kv_cols // HEAD
    group_size = head_count // kv_count
    gain_float = norm_gain.astype(jnp.float32)
    floats = lax.all_gather(tokens, "tp", axis=0, tiled=True).astype(jnp.float32)
    normed = (
        floats * lax.rsqrt(jnp.mean(floats * floats, axis=-1, keepdims=True) + 1e-06) * gain_float
    ).astype(jnp.bfloat16)
    query_part = jnp.dot(normed, w_query, preferred_element_type=jnp.float32).astype(jnp.bfloat16)
    key_part = jnp.dot(normed, w_key, preferred_element_type=jnp.float32).astype(jnp.bfloat16)
    value_part = jnp.dot(normed, w_value, preferred_element_type=jnp.float32).astype(jnp.bfloat16)
    value_glu = jnp.dot(normed, w_conv_value, preferred_element_type=jnp.float32)
    gate_glu = jnp.dot(normed, w_conv_gate, preferred_element_type=jnp.float32)
    glu_part = (value_glu * jax.nn.sigmoid(gate_glu)).astype(jnp.bfloat16)
    joined = jnp.concatenate([query_part, key_part, value_part, glu_part], axis=1)
    local_rows = joined.shape[0]
    query = joined[:, :query_cols]
    key_rows = joined[:, query_cols : query_cols + kv_cols]
    value_rows = joined[:, query_cols + kv_cols : query_cols + 2 * kv_cols]
    glu = joined[:, query_cols + 2 * kv_cols :]
    offset = lax.axis_index("sp") * local_rows
    query_places = offset + jnp.arange(local_rows, dtype=jnp.int32)
    query_gate = lax.dynamic_slice_in_dim(cum_gate, offset, local_rows, 0).T
    query_groups = query.reshape(local_rows, kv_count, group_size, HEAD)
    scale = 1.0 / math.sqrt(HEAD)

    def attend_block(state, key_block, value_block, key_start):
        run_max, run_sum, run_acc = state
        span = key_block.shape[0]
        key_heads = key_block.reshape(span, kv_count, HEAD)
        value_heads = value_block.reshape(span, kv_count, HEAD)
        scores = (
            jnp.einsum(
                "tkgd,skd->kgts", query_groups, key_heads, preferred_element_type=jnp.float32
            ).reshape(head_count, local_rows, span)
            * scale
        )
        key_gate = lax.dynamic_slice_in_dim(cum_gate, key_start, span, 0).T
        logits = scores + query_gate[:, :, None] - key_gate[:, None, :]
        key_places = key_start + jnp.arange(span, dtype=jnp.int32)
        allowed = (key_places[None, :] <= query_places[:, None])[None]
        logits = jnp.where(allowed, logits, -1e30)
        new_max = jnp.maximum(run_max, jnp.max(logits, axis=-1))
        weights = jnp.where(allowed, jnp.exp(logits - new_max[:, :, None]), 0.0)
        factor = jnp.exp(run_max - new_max)
        new_sum = run_sum * factor + jnp.sum(weights, axis=-1)
        grouped = weights.astype(jnp.bfloat16).reshape(kv_count, group_size, local_rows, span)
        product = jnp.einsum(
            "kgts,skd->kgtd", grouped, value_heads, preferred_element_type=jnp.float32
        ).reshape(head_count, local_rows, HEAD)
        new_acc = run_acc * factor[:, :, None] + product
        return (new_max, new_sum, new_acc)

    shard_rows = key_rows.shape[0]

    def fold_keys(state, pieces, start):
        key_piece, value_piece = pieces
        span = key_piece.shape[0]
        shards_in = span // shard_rows
        group = 1
        for divisor in range(1, shards_in + 1):
            if shards_in % divisor == 0 and divisor * shard_rows <= 2048:
                group = divisor
        block = group * shard_rows
        if block >= span:
            return attend_block(state, key_piece, value_piece, start)
        key_blocks = key_piece.reshape(span // block, block, kv_cols)
        value_blocks = value_piece.reshape(span // block, block, kv_cols)
        firsts = start + block * jnp.arange(span // block, dtype=jnp.int32)

        def step_block(inner, items):
            return (attend_block(inner, items[0], items[1], items[2]), None)

        result, unused = lax.scan(step_block, state, (key_blocks, value_blocks, firsts))
        return result

    start_state = (
        jnp.full((head_count, local_rows), -1e30, jnp.float32),
        jnp.zeros((head_count, local_rows), jnp.float32),
        jnp.zeros((head_count, local_rows, HEAD), jnp.float32),
    )
    run_max, run_sum, run_acc = fold_keys(
        start_state,
        (
            lax.all_gather(key_rows, "sp", axis=0, tiled=True),
            lax.all_gather(value_rows, "sp", axis=0, tiled=True),
        ),
        jnp.int32(0),
    )
    attended = jnp.transpose(
        (run_acc / run_sum[:, :, None]).astype(jnp.bfloat16), (1, 0, 2)
    ).reshape(local_rows, query_cols)
    rim = shifted(glu[local_rows - (KW - 1) :], "sp", 1)
    padded = jnp.concatenate([rim, glu], axis=0).astype(jnp.float32)
    taps = conv_taps.astype(jnp.float32)
    conv = jnp.zeros((local_rows, conv_cols), jnp.float32)
    for shift_tap in range(KW):
        conv = conv + taps[shift_tap][None, :] * padded[shift_tap : shift_tap + local_rows]
    first_sum, square_sum = lax.psum((jnp.sum(conv, axis=1), jnp.sum(conv * conv, axis=1)), "tp")
    mean_c = (first_sum / CONV)[:, None]
    var_c = (square_sum / CONV)[:, None] - mean_c * mean_c
    shaped = (conv - mean_c) * lax.rsqrt(var_c + 1e-05) * conv_gain.astype(
        jnp.float32
    ) + conv_bias.astype(jnp.float32)
    conv_act = jax.nn.silu(shaped).astype(jnp.bfloat16)
    att_weight, conv_weight = (
        lax.all_gather(w_out_att, "sp", axis=1, tiled=True),
        lax.all_gather(w_out_conv, "sp", axis=1, tiled=True),
    )
    terms = jnp.dot(attended, att_weight, preferred_element_type=jnp.float32) + jnp.dot(
        conv_act, conv_weight, preferred_element_type=jnp.float32
    )
    return lax.psum_scatter(terms.astype(jnp.bfloat16), "tp", scatter_dimension=1, tiled=True)


F32 = jnp.float32
BF16 = jnp.bfloat16


def fused_kernel(
    n_sp,
    n_tp,
    tokens_h,
    gain_h,
    wq_h,
    wk_h,
    wv_h,
    wcv_h,
    wcg_h,
    taps_h,
    cgain_h,
    cbias_h,
    gate_h,
    woa_h,
    woc_h,
    out_r,
    tok,
    normed,
    wq,
    wk,
    wv,
    wcv,
    wcg,
    taps,
    gate,
    gain_v,
    cgain_v,
    cbias_v,
    wbuf,
    kv,
    pad,
    rim_out,
    rim_in,
    stat,
    act,
    pair_out,
    pair_in,
    cross_out,
    cross_in,
    local_sem,
    tok_send,
    tok_recv,
    w_send,
    w_recv,
    kv_send,
    kv_recv,
    rim_sem,
    stat_send,
    stat_recv,
    out_send,
    out_recv,
):
    s = lax.axis_index("sp")
    t = lax.axis_index("tp")
    rem = lax.rem
    core = t + 1 - 2 * rem(t, 2)
    cross = rem(t + 2, n_tp)
    diag = rem(core + 2, n_tp)
    side = s + 1 - 2 * rem(s, 2)
    up = rem(s + 2, n_sp)
    down = rem(s + n_sp - 2, n_sp)
    after = rem(s + 1, n_sp)
    other = rem(s + n_sp - 1 + 2 * rem(s, 2), n_sp)

    rows_in = tokens_h.shape[0]
    rows = rows_in * n_tp
    head_count = gate_h.shape[0]
    ccols = wcv_h.shape[1]
    half = woa_h.shape[0]

    def local(src, dst, index):
        copy = pltpu.make_async_copy(src, dst, local_sem.at[index])
        copy.start()
        return copy

    def remote(src, dst, send, recv, where):
        return pltpu.make_async_remote_copy(
            src_ref=src,
            dst_ref=dst,
            send_sem=send,
            recv_sem=recv,
            device_id=where,
            device_id_type=pl.DeviceIdType.MESH,
        )

    own_tok = local(tokens_h, tok.at[t], 0)
    own_a = local(woa_h, wbuf.at[s, pl.ds(0, half)], 1)
    own_b = local(woc_h, wbuf.at[s, pl.ds(half, half)], 2)
    load_gate = local(gate_h, gate, 3)
    load_k = local(wk_h, wk, 4)
    load_v = local(wv_h, wv, 5)
    load_cv = local(wcv_h, wcv, 6)
    load_cg = local(wcg_h, wcg, 7)
    load_q = local(wq_h, wq, 8)
    load_taps = local(taps_h, taps, 9)
    load_gain = local(gain_h, gain_v, 10)
    load_cgain = local(cgain_h, cgain_v, 11)
    load_cbias = local(cbias_h, cbias_v, 12)

    barrier = pltpu.get_barrier_semaphore()
    greeted = [{"tp": core}, {"tp": cross}, {"tp": diag}]
    greeted += [{"sp": side}, {"sp": up}, {"sp": down}, {"sp": other}]
    for peer in greeted:
        pl.semaphore_signal(
            barrier, inc=1, device_id=peer, device_id_type=pl.DeviceIdType.MESH
        )
    own_tok.wait()
    pl.semaphore_wait(barrier, len(greeted))

    sent = []

    def go(copy, when=None):
        if when is None:
            copy.start()
        else:
            pl.when(when)(copy.start)
        sent.append((copy, when))

    def tok_copy(slot, number, where):
        return remote(tok.at[slot], tok.at[slot], tok_send.at[number], tok_recv.at[slot], where)

    go(tok_copy(t, 0, {"tp": cross}))
    go(tok_copy(t, 1, {"tp": core}))

    z = s // 2
    last = n_sp // 2 - 1

    def w_copy(slot, part, number, where):
        piece = wbuf.at[slot, pl.ds(part * half, half)]
        return remote(piece, piece, w_send.at[number], w_recv.at[slot, part], where)

    def kv_copy(slot, part, number, where):
        piece = kv.at[part, pl.ds(pl.multiple_of(slot * rows, rows), rows)]
        return remote(piece, piece, kv_send.at[number], kv_recv.at[slot, part], where)

    class Gather:
        def __init__(self, copy_of, both_ways):
            self.copy_of, self.both, self.count = copy_of, both_ways, 0

        def send(self, slot, part, where, when=None):
            go(self.copy_of(slot, part, self.count, {"sp": where}), when)
            self.count += 1

        def wait(self, slot, part, when=None):
            copy = self.copy_of(slot, part, 0, {"sp": side})
            if when is None:
                copy.wait_recv()
            else:
                pl.when(when)(copy.wait_recv)

        def own(self):
            for part in range(2):
                self.send(s, part, up, z < last)
                if self.both:
                    self.send(s, part, down, z > 0)
                self.send(s, part, side)

        def pass_on(self, distance, part):
            below = rem(s + n_sp - 2 * distance, n_sp)
            above = rem(s + 2 * distance, n_sp)
            self.wait(below, part, z >= distance)
            self.send(below, part, up, (z >= distance) & (z < last))
            if distance > 1 or part == 0:
                self.send(below, part, side, z >= distance)
            if self.both:
                self.wait(above, part, z + distance <= last)
                self.send(above, part, down, (z + distance <= last) & (z > 0))
                if distance > 1 or part == 0:
                    self.send(above, part, side, z + distance <= last)
            if distance == 1:
                self.wait(side, part)
                if part == 1:
                    self.send(side, part, up, z < last)
                    if self.both:
                        self.send(side, part, down, z > 0)

        def end(self):
            for distance in range(1, last + 1):
                for part in range(2):
                    self.wait(rem(side + n_sp - 2 * distance, n_sp), part, z >= distance)
                    if self.both:
                        self.wait(
                            rem(side + 2 * distance, n_sp), part, z + distance <= last
                        )

    w_gather = Gather(w_copy, True)
    kv_gather = Gather(kv_copy, False)

    own_a.wait()
    own_b.wait()
    w_gather.own()
    for later in range(1, last + 1):

        @pl.when(later > z)
        def _():
            blank = pl.ds(later * 2 * rows, 2 * rows)
            kv[:, blank, :] = jnp.zeros((2, 2 * rows, kv.shape[2]), BF16)


    diagonal = lax.broadcasted_iota(jnp.int32, (rows, rows), 0) == lax.broadcasted_iota(
        jnp.int32, (rows, rows), 1
    )

    def to_lanes(column):
        return jnp.sum(jnp.where(diagonal, column, 0.0), axis=0, keepdims=True)

    def to_sublanes(row):
        return jnp.sum(jnp.where(diagonal, row, 0.0), axis=1, keepdims=True)

    load_gain.wait()
    gain = gain_v[...].astype(F32)[None, :]

    def norm_rows(slot):
        floats = tok[slot].astype(F32)
        scaled = floats * lax.rsqrt(jnp.mean(floats * floats, axis=-1, keepdims=True) + 1e-06)
        normed[pl.ds(pl.multiple_of(slot * rows_in, rows_in), rows_in), :] = (
            scaled * gain
        ).astype(BF16)

    norm_rows(t)
    tok_copy(core, 0, {"tp": core}).wait_recv()
    norm_rows(core)
    tok_copy(cross, 0, {"tp": core}).wait_recv()
    go(tok_copy(cross, 2, {"tp": core}))
    norm_rows(cross)
    tok_copy(diag, 0, {"tp": core}).wait_recv()
    norm_rows(diag)

    def project(weight):
        return jnp.dot(normed[...], weight[...], preferred_element_type=F32)

    own_rows = pl.ds(pl.multiple_of(s * rows, rows), rows)
    load_k.wait()
    load_v.wait()
    kv[0, own_rows, :] = project(wk).astype(BF16)
    kv[1, own_rows, :] = project(wv).astype(BF16)
    kv_gather.own()
    w_gather.pass_on(1, 0)

    load_cv.wait()
    load_cg.wait()
    glu = (project(wcv) * jax.nn.sigmoid(project(wcg))).astype(BF16)
    rim = rim_out.shape[0]
    rim_out[...] = glu[rows - rim :]
    rim_copy = remote(rim_out, rim_in, rim_sem.at[0], rim_sem.at[1], {"sp": after})
    go(rim_copy)
    pad[pl.ds(rim, rows), :] = glu.astype(F32)

    kv_gather.pass_on(1, 0)
    kv_gather.pass_on(1, 1)
    w_gather.pass_on(1, 1)

    for part in range(2):
        kv_gather.pass_on(2, part)
    for part in range(2):
        w_gather.pass_on(2, part)
    load_q.wait()
    query = project(wq).astype(BF16)

    load_taps.wait()
    rim_copy.wait_recv()
    pad[pl.ds(0, rim), :] = jnp.where(s == 0, 0.0, rim_in[...].astype(F32))
    lead = rim - (KW - 1)
    conv = jnp.zeros((rows, ccols), F32)
    for tap in range(KW):
        conv = conv + taps[pl.ds(tap, 1), :].astype(F32) * pad[pl.ds(lead + tap, rows), :]
    stat[t] = jnp.zeros(stat.shape[1:], F32)
    stat[t, pl.ds(0, 1), :] = to_lanes(jnp.sum(conv, axis=1, keepdims=True))
    stat[t, pl.ds(1, 1), :] = to_lanes(jnp.sum(conv * conv, axis=1, keepdims=True))

    def stat_copy(slot, number, where):
        return remote(stat.at[slot], stat.at[slot], stat_send.at[number], stat_recv.at[slot], where)

    for number, peer in enumerate((core, cross, diag)):
        go(stat_copy(t, number, {"tp": peer}))


    load_cgain.wait()
    load_cbias.wait()
    for peer in (core, cross, diag):
        stat_copy(peer, 0, {"tp": core}).wait_recv()
    totals = stat[0]
    for peer in range(1, n_tp):
        totals = totals + stat[peer]
    channels = n_tp * ccols
    mean_c = to_sublanes(totals[0:1]) / channels
    var_c = to_sublanes(totals[1:2]) / channels - mean_c * mean_c
    shaped = (conv - mean_c) * lax.rsqrt(var_c + 1e-05) * cgain_v[...].astype(F32)[
        None, :
    ] + cbias_v[...].astype(F32)[None, :]
    act[:, pl.ds(half, ccols)] = (shaped / (1.0 + jnp.exp(-shaped))).astype(BF16)

    for part in range(2):
        kv_gather.pass_on(3, part)
    kv_gather.end()
    for part in range(2):
        w_gather.pass_on(3, part)
    length = kv.shape[1]
    scale = 1.0 / math.sqrt(HEAD)
    key_places = lax.broadcasted_iota(jnp.int32, (rows, length), 1)
    allowed = key_places <= s * rows + lax.broadcasted_iota(jnp.int32, (rows, length), 0)
    load_gate.wait()
    for head in range(head_count):
        scores = (
            lax.dot_general(
                query[:, head * HEAD : (head + 1) * HEAD],
                kv[0],
                (((1,), (1,)), ((), ())),
                preferred_element_type=F32,
            )
            * scale
        )
        query_gate = to_sublanes(gate[pl.ds(head, 1), own_rows])
        logits = scores + query_gate - gate[pl.ds(head, 1), :]
        logits = jnp.where(allowed, logits, -1e30)
        weights = jnp.exp(logits - jnp.max(logits, axis=-1, keepdims=True))
        denom = jnp.sum(weights, axis=-1, keepdims=True)
        numer = jnp.dot(weights.astype(BF16), kv[1], preferred_element_type=F32)
        act[:, pl.ds(head * HEAD, HEAD)] = (numer / denom).astype(BF16)

    w_gather.end()

    per = n_sp // n_tp
    wide = wbuf.shape[2]

    def terms(chunk, block):
        return jnp.dot(act[...], wbuf[chunk * per + block], preferred_element_type=F32)

    x = t // 2
    for step, column in enumerate((1 - x, x)):
        chunk = 2 * column + rem(core, 2)
        for block in range(per):
            pair_out[step, :, pl.ds(block * wide, wide)] = terms(chunk, block).astype(BF16)
        go(
            remote(
                pair_out.at[step],
                pair_in.at[step],
                out_send.at[step],
                out_recv.at[step],
                {"tp": core},
            )
        )
    mine = [terms(2 * (1 - x) + rem(t, 2), block) for block in range(per)]
    remote(
        pair_out.at[0], pair_in.at[0], out_send.at[0], out_recv.at[0], {"tp": core}
    ).wait_recv()
    for block in range(per):
        piece = pl.ds(block * wide, wide)
        cross_out[:, piece] = (mine[block] + pair_in[0, :, piece].astype(F32)).astype(BF16)
    cross_copy = remote(cross_out, cross_in, out_send.at[2], out_recv.at[2], {"tp": cross})
    go(cross_copy)
    mine = [terms(t, block) for block in range(per)]
    remote(
        pair_out.at[1], pair_in.at[1], out_send.at[1], out_recv.at[1], {"tp": core}
    ).wait_recv()
    for block in range(per):
        mine[block] = mine[block] + pair_in[1, :, pl.ds(block * wide, wide)].astype(F32)
    cross_copy.wait_recv()
    for block in range(per):
        piece = pl.ds(block * wide, wide)
        out_r[:, piece] = (mine[block] + cross_in[:, piece].astype(F32)).astype(BF16)
    for copy, when in sent:
        if when is None:
            copy.wait_send()
        else:
            pl.when(when)(copy.wait_send)


def fused(n_sp, n_tp, *args):
    tokens, gain, wq, wk, wv, wcv, wcg, taps, cgain, cbias, gate, woa, woc = args
    rows_in, width = tokens.shape
    rows = rows_in * n_tp
    rim = -(-(KW - 1) // 16) * 16
    wide = woa.shape[1]
    out_wide = wide * n_sp // n_tp
    both = woa.shape[0] + woc.shape[0]
    hbm = pl.BlockSpec(memory_space=pltpu.HBM)
    vmem = pl.BlockSpec(memory_space=pltpu.VMEM)
    dma = pltpu.SemaphoreType.DMA
    scratch = [
        pltpu.VMEM((n_tp, rows_in, width), BF16),
        pltpu.VMEM((rows, width), BF16),
        *[pltpu.VMEM(w.shape, w.dtype) for w in (wq, wk, wv, wcv, wcg, taps)],
        pltpu.VMEM(gate.shape[::-1], F32),
        pltpu.VMEM(gain.shape, BF16),
        pltpu.VMEM(cgain.shape, BF16),
        pltpu.VMEM(cbias.shape, BF16),
        pltpu.VMEM((n_sp, both, wide), BF16),
        pltpu.VMEM((2, n_sp * rows, wk.shape[1]), BF16),
        pltpu.VMEM((rim + rows, wcv.shape[1]), F32),
        pltpu.VMEM((rim, wcv.shape[1]), BF16),
        pltpu.VMEM((rim, wcv.shape[1]), BF16),
        pltpu.VMEM((n_tp, 8, rows), F32),
        pltpu.VMEM((rows, both), BF16),
        pltpu.VMEM((2, rows, out_wide), BF16),
        pltpu.VMEM((2, rows, out_wide), BF16),
        pltpu.VMEM((rows, out_wide), BF16),
        pltpu.VMEM((rows, out_wide), BF16),
        dma((13,)),
        dma((3,)),
        dma((n_tp,)),
        dma((40,)),
        dma((n_sp, 2)),
        dma((40,)),
        dma((n_sp, 2)),
        dma((2,)),
        dma((3,)),
        dma((n_tp,)),
        dma((3,)),
        dma((3,)),
    ]
    return pl.pallas_call(
        functools.partial(fused_kernel, n_sp, n_tp),
        out_shape=jax.ShapeDtypeStruct((rows, out_wide), BF16),
        in_specs=[hbm] * 13,
        out_specs=vmem,
        scratch_shapes=scratch,
        compiler_params=pltpu.CompilerParams(
            collective_id=0, has_side_effects=True, vmem_limit_bytes=67_043_328
        ),
    )(
        tokens, gain, wq, wk, wv, wcv, wcg, taps,
        cgain, cbias, gate.T, woa, woc,
    )


def layer(sizes, *args):
    n_sp, n_tp = sizes["sp"], sizes["tp"]
    tokens, wq, wk, wcv, woa, woc = (args[k] for k in (0, 2, 3, 5, 11, 12))
    fits = (
        n_sp == 8
        and n_tp == 4
        and tokens.shape[0] * n_tp == HEAD
        and wk.shape[1] == HEAD
        and woa.shape[1] % HEAD == 0
        and woa.shape == woc.shape
        and wq.shape[1] == wcv.shape[1] == woa.shape[0]
    )
    if fits:
        return fused(n_sp, n_tp, *args)
    return shards(*args)


def solution(mesh):
    return jax.shard_map(
        functools.partial(layer, dict(mesh.shape)),
        mesh=mesh,
        in_specs=(
            P(("sp", "tp"), None),
            P(),
            P(None, "tp"),
            P(None, "tp"),
            P(None, "tp"),
            P(None, "tp"),
            P(None, "tp"),
            P(None, "tp"),
            P("tp"),
            P("tp"),
            P(None, "tp"),
            P("tp", "sp"),
            P("tp", "sp"),
        ),
        out_specs=P("sp", "tp"),
        check_vma=False,
    )
```

profile of v0, /device:TPU:24, one launch (start us, length us, event | category | flops | bytes accessed | tf_op | source)
XLA Modules:
  0.0 44.0 jit_solution(10531289224122537705)
XLA Ops:
  0.0 42.4 %shard_map.127 = bf16[128,512]{1,0:T(8,128)(2,1)} custom-call(bf16[32,2048]{1,0:T(8,128)(2,1)} %tokens_h.1, bf16[2048]{0:T(1024)(128)(2,1)} %gain_h.1, bf16[2048,256]{1,0:T(8,128)(2,1)} %wq_h.1, bf16[2048,128]{1,0:T(8,128)(2,1)} %wk_h.1, bf16[2048,128]{1,0:T(8,128)(2,1)} %wv_h.1, bf16[2048,256]{1,0:T(8,128)(2,1)} %wcv_h.1, bf16[2048,256]{1,0:T(8,128)(2,1)} %wcg_h.1, ...), custom_call_target="tpu_custom_call" | custom-call | tf_op jit(solution)/shard_map/pallas_call | solution.py:571
  42.4 1.6 %copy.15 = bf16[128,512]{1,0:T(8,128)(2,1)} copy(bf16[128,512]{1,0:T(8,128)(2,1)} %shard_map.127) | data formatting | bytes 262144
where the time goes:
time: 44.1 us; the launch traced here: 44 us
  Pallas kernels  42.4 us (96%)
  local copies, waits for them, and re-layouts  1.57 us (4%)
    pallas_call x1, Pallas kernels, fused(): pl.pallas_call(functools.partial(fused_kernel, n_sp, n_tp), out_shape=jax...  42.4 us
    unnamed x1, local copies, waits for them, and re-layouts  1.57 us

commit v1 on v0

--- a/solution.py
+++ b/solution.py
@@ -570,12 +570,12 @@
     ]
     return pl.pallas_call(
         functools.partial(fused_kernel, n_sp, n_tp),
-        out_shape=jax.ShapeDtypeStruct((rows, out_wide), BF16),
+        out_shape=pltpu.VMEM((rows, out_wide), BF16),
         in_specs=[hbm] * 13,
         out_specs=vmem,
         scratch_shapes=scratch,
         compiler_params=pltpu.CompilerParams(
-            collective_id=0, has_side_effects=True, vmem_limit_bytes=67_043_328
+            collective_id=0, has_side_effects=True, vmem_limit_bytes=66_846_720
         ),
     )(
         tokens, gain, wq, wk, wv, wcv, wcg, taps,

time: 44.1 us -> 42.6 us (0.966)
  local copies, waits for them, and re-layouts: 1.57 us -> 0.66 us
  Pallas kernels: 42.4 us -> 41.8 us
    unnamed x1, local copies, waits for them, and re-layouts: 1.57 us -> 0.66 us
    pallas_call x1, Pallas kernels: 42.4 us -> 41.8 us  [fused(): pl.pallas_call(functools.partial(fused_kernel, n_sp, n_tp), out_shape=plt...]
where the time goes in v1:
time: 42.6 us; the launch traced here: 42.4 us
  Pallas kernels  41.8 us (98%)
  local copies, waits for them, and re-layouts  0.66 us (2%)
    pallas_call x1, Pallas kernels, fused(): pl.pallas_call(functools.partial(fused_kernel, n_sp, n_tp), out_shape=plt...  41.8 us

profile of v1, /device:TPU:24, one launch (start us, length us, event | category | flops | bytes accessed | tf_op | source)
XLA Modules:
  0.0 42.4 jit_solution(2714927333500293131)
XLA Ops:
  0.0 41.8 %shard_map.127 = bf16[128,512]{1,0:T(8,128)(2,1)S(1)} custom-call(bf16[32,2048]{1,0:T(8,128)(2,1)} %tokens_h.1, bf16[2048]{0:T(1024)(128)(2,1)} %gain_h.1, bf16[2048,256]{1,0:T(8,128)(2,1)} %wq_h.1, bf16[2048,128]{1,0:T(8,128)(2,1)} %wk_h.1, bf16[2048,128]{1,0:T(8,128)(2,1)} %wv_h.1, bf16[2048,256]{1,0:T(8,128)(2,1)} %wcv_h.1, bf16[2048,256]{1,0:T(8,128)(2,1)} %wcg_h.1, ...), custom_call_target="tpu_custom_call" | custom-call | tf_op jit(solution)/shard_map/pallas_call | solution.py:571
  41.8 0.7 %copy.15 = bf16[128,512]{1,0:T(8,128)(2,1)} copy(bf16[128,512]{1,0:T(8,128)(2,1)S(1)} %shard_map.127) | data formatting | bytes 262144

commit v2 on v1

v2 whole, which is shorter than its diff:
```python
import functools
import math

import jax
import jax.numpy as jnp
from jax import lax
from jax.experimental import pallas as pl
from jax.experimental.pallas import tpu as pltpu
from jax.sharding import PartitionSpec as P

HEAD = 128
CONV = 1024
KW = 31


def shifted(array, axis, by):
    peers = lax.axis_size(axis)
    pairs = [(i, i + by) for i in range(peers) if 0 <= i + by < peers]
    return lax.ppermute(array, axis, pairs)


def shards(
    tokens,
    norm_gain,
    w_query,
    w_key,
    w_value,
    w_conv_value,
    w_conv_gate,
    conv_taps,
    conv_gain,
    conv_bias,
    cum_gate,
    w_out_att,
    w_out_conv,
):
    query_cols = w_query.shape[1]
    kv_cols = w_key.shape[1]
    conv_cols = w_conv_value.shape[1]
    head_count = query_cols // HEAD
    kv_count = kv_cols // HEAD
    group_size = head_count // kv_count
    gain_float = norm_gain.astype(jnp.float32)
    floats = lax.all_gather(tokens, "tp", axis=0, tiled=True).astype(jnp.float32)
    normed = (
        floats * lax.rsqrt(jnp.mean(floats * floats, axis=-1, keepdims=True) + 1e-06) * gain_float
    ).astype(jnp.bfloat16)
    query_part = jnp.dot(normed, w_query, preferred_element_type=jnp.float32).astype(jnp.bfloat16)
    key_part = jnp.dot(normed, w_key, preferred_element_type=jnp.float32).astype(jnp.bfloat16)
    value_part = jnp.dot(normed, w_value, preferred_element_type=jnp.float32).astype(jnp.bfloat16)
    value_glu = jnp.dot(normed, w_conv_value, preferred_element_type=jnp.float32)
    gate_glu = jnp.dot(normed, w_conv_gate, preferred_element_type=jnp.float32)
    glu_part = (value_glu * jax.nn.sigmoid(gate_glu)).astype(jnp.bfloat16)
    joined = jnp.concatenate([query_part, key_part, value_part, glu_part], axis=1)
    local_rows = joined.shape[0]
    query = joined[:, :query_cols]
    key_rows = joined[:, query_cols : query_cols + kv_cols]
    value_rows = joined[:, query_cols + kv_cols : query_cols + 2 * kv_cols]
    glu = joined[:, query_cols + 2 * kv_cols :]
    offset = lax.axis_index("sp") * local_rows
    query_places = offset + jnp.arange(local_rows, dtype=jnp.int32)
    query_gate = lax.dynamic_slice_in_dim(cum_gate, offset, local_rows, 0).T
    query_groups = query.reshape(local_rows, kv_count, group_size, HEAD)
    scale = 1.0 / math.sqrt(HEAD)

    def attend_block(state, key_block, value_block, key_start):
        run_max, run_sum, run_acc = state
        span = key_block.shape[0]
        key_heads = key_block.reshape(span, kv_count, HEAD)
        value_heads = value_block.reshape(span, kv_count, HEAD)
        scores = (
            jnp.einsum(
                "tkgd,skd->kgts", query_groups, key_heads, preferred_element_type=jnp.float32
            ).reshape(head_count, local_rows, span)
            * scale
        )
        key_gate = lax.dynamic_slice_in_dim(cum_gate, key_start, span, 0).T
        logits = scores + query_gate[:, :, None] - key_gate[:, None, :]
        key_places = key_start + jnp.arange(span, dtype=jnp.int32)
        allowed = (key_places[None, :] <= query_places[:, None])[None]
        logits = jnp.where(allowed, logits, -1e30)
        new_max = jnp.maximum(run_max, jnp.max(logits, axis=-1))
        weights = jnp.where(allowed, jnp.exp(logits - new_max[:, :, None]), 0.0)
        factor = jnp.exp(run_max - new_max)
        new_sum = run_sum * factor + jnp.sum(weights, axis=-1)
        grouped = weights.astype(jnp.bfloat16).reshape(kv_count, group_size, local_rows, span)
        product = jnp.einsum(
            "kgts,skd->kgtd", grouped, value_heads, preferred_element_type=jnp.float32
        ).reshape(head_count, local_rows, HEAD)
        new_acc = run_acc * factor[:, :, None] + product
        return (new_max, new_sum, new_acc)

    shard_rows = key_rows.shape[0]

    def fold_keys(state, pieces, start):
        key_piece, value_piece = pieces
        span = key_piece.shape[0]
        shards_in = span // shard_rows
        group = 1
        for divisor in range(1, shards_in + 1):
            if shards_in % divisor == 0 and divisor * shard_rows <= 2048:
                group = divisor
        block = group * shard_rows
        if block >= span:
            return attend_block(state, key_piece, value_piece, start)
        key_blocks = key_piece.reshape(span // block, block, kv_cols)
        value_blocks = value_piece.reshape(span // block, block, kv_cols)
        firsts = start + block * jnp.arange(span // block, dtype=jnp.int32)

        def step_block(inner, items):
            return (attend_block(inner, items[0], items[1], items[2]), None)

        result, unused = lax.scan(step_block, state, (key_blocks, value_blocks, firsts))
        return result

    start_state = (
        jnp.full((head_count, local_rows), -1e30, jnp.float32),
        jnp.zeros((head_count, local_rows), jnp.float32),
        jnp.zeros((head_count, local_rows, HEAD), jnp.float32),
    )
    run_max, run_sum, run_acc = fold_keys(
        start_state,
        (
            lax.all_gather(key_rows, "sp", axis=0, tiled=True),
            lax.all_gather(value_rows, "sp", axis=0, tiled=True),
        ),
        jnp.int32(0),
    )
    attended = jnp.transpose(
        (run_acc / run_sum[:, :, None]).astype(jnp.bfloat16), (1, 0, 2)
    ).reshape(local_rows, query_cols)
    rim = shifted(glu[local_rows - (KW - 1) :], "sp", 1)
    padded = jnp.concatenate([rim, glu], axis=0).astype(jnp.float32)
    taps = conv_taps.astype(jnp.float32)
    conv = jnp.zeros((local_rows, conv_cols), jnp.float32)
    for shift_tap in range(KW):
        conv = conv + taps[shift_tap][None, :] * padded[shift_tap : shift_tap + local_rows]
    first_sum, square_sum = lax.psum((jnp.sum(conv, axis=1), jnp.sum(conv * conv, axis=1)), "tp")
    mean_c = (first_sum / CONV)[:, None]
    var_c = (square_sum / CONV)[:, None] - mean_c * mean_c
    shaped = (conv - mean_c) * lax.rsqrt(var_c + 1e-05) * conv_gain.astype(
        jnp.float32
    ) + conv_bias.astype(jnp.float32)
    conv_act = jax.nn.silu(shaped).astype(jnp.bfloat16)
    att_weight, conv_weight = (
        lax.all_gather(w_out_att, "sp", axis=1, tiled=True),
        lax.all_gather(w_out_conv, "sp", axis=1, tiled=True),
    )
    terms = jnp.dot(attended, att_weight, preferred_element_type=jnp.float32) + jnp.dot(
        conv_act, conv_weight, preferred_element_type=jnp.float32
    )
    return lax.psum_scatter(terms.astype(jnp.bfloat16), "tp", scatter_dimension=1, tiled=True)


F32 = jnp.float32
BF16 = jnp.bfloat16


def fused_kernel(
    n_sp,
    n_tp,
    tokens_h,
    gain_h,
    wq_h,
    wk_h,
    wv_h,
    wcv_h,
    wcg_h,
    taps_h,
    cgain_h,
    cbias_h,
    gate_h,
    woa_h,
    woc_h,
    out_r,
    tok,
    normed,
    wq,
    wk,
    wv,
    wcv,
    wcg,
    taps,
    gate,
    gain_v,
    cgain_v,
    cbias_v,
    wbuf,
    kv,
    pad,
    rim_out,
    rim_in,
    stat,
    act,
    acc,
    pair_out,
    pair_in,
    sum_out,
    sum_in,
    local_sem,
    tok_send,
    tok_recv,
    w_send,
    w_recv,
    kv_send,
    kv_recv,
    rim_sem,
    stat_send,
    stat_recv,
    act_send,
    act_recv,
    pair_send,
    pair_recv,
    sum_send,
    sum_recv,
):
    scope = jax.named_scope
    s = lax.axis_index("sp")
    t = lax.axis_index("tp")
    rem = lax.rem
    last = n_sp // 2 - 1
    core = t + 1 - 2 * rem(t, 2)
    cross = rem(t + 2, n_tp)
    diag = rem(core + 2, n_tp)
    y = rem(s, 2)
    z = s // 2
    side = s + 1 - 2 * y
    mate = (z + 1 - 2 * rem(z, 2)) * 2 + y
    far = (last - z) * 2 + y
    after = rem(s + 1, n_sp)
    up = rem(s + 2, n_sp)
    up_two = rem(s + 4, n_sp)
    home = (t == z) | (t == last - z)
    near_mine = rem(t, 2) == rem(z, 2)

    rows_in = tokens_h.shape[0]
    rows = rows_in * n_tp
    head_count = gate_h.shape[0]
    ccols = wcv_h.shape[1]
    half = woa_h.shape[0]
    wide = wbuf.shape[2]
    pieces = w_recv.shape[1]
    deep = wbuf.shape[1] // pieces

    def local(src, dst, index):
        copy = pltpu.make_async_copy(src, dst, local_sem.at[index])
        copy.start()
        return copy

    def remote(src, dst, send, recv, where):
        return pltpu.make_async_remote_copy(
            src_ref=src,
            dst_ref=dst,
            send_sem=send,
            recv_sem=recv,
            device_id=where,
            device_id_type=pl.DeviceIdType.MESH,
        )

    own_tok = local(tokens_h, tok.at[t], 0)
    own_a = local(woa_h, wbuf.at[y, pl.ds(0, half)], 1)
    own_b = local(woc_h, wbuf.at[y, pl.ds(half, half)], 2)
    load_gate = local(gate_h, gate, 3)
    load_gain = local(gain_h, gain_v, 10)
    load_k = local(wk_h, wk, 4)
    load_v = local(wv_h, wv, 5)
    load_cv = local(wcv_h, wcv, 6)
    load_cg = local(wcg_h, wcg, 7)
    load_q = local(wq_h, wq, 8)
    load_taps = local(taps_h, taps, 9)
    load_cgain = local(cgain_h, cgain_v, 11)
    load_cbias = local(cbias_h, cbias_v, 12)

    with scope("barrier"):
        barrier = pltpu.get_barrier_semaphore()
        greeted = [{"tp": core}, {"tp": cross}, {"tp": diag}, {"sp": mate, "tp": cross}]
        greeted += [{"sp": rem(s + by, n_sp)} for by in range(1, n_sp)]
        for peer in greeted:
            pl.semaphore_signal(
                barrier, inc=1, device_id=peer, device_id_type=pl.DeviceIdType.MESH
            )
        own_tok.wait()
        pl.semaphore_wait(barrier, len(greeted))

    sent = []

    def go(copy, when=None):
        if when is None:
            copy.start()
        else:
            pl.when(when)(copy.start)
        sent.append((copy, when))

    tok_half = rows_in // 2

    def tok_copy(slot, part, number, where):
        piece = tok.at[slot, pl.ds(part * tok_half, tok_half)]
        return remote(piece, piece, tok_send.at[number], tok_recv.at[slot, part], where)

    for part in range(2):
        go(tok_copy(t, part, part, {"tp": cross}))
    for part in range(2):
        go(tok_copy(t, part, 2 + part, {"tp": core}))

    def w_copy(source, target, piece, number, where):
        span = pl.ds(piece * deep, deep)
        return remote(
            wbuf.at[source, span],
            wbuf.at[target, span],
            w_send.at[number],
            w_recv.at[target, piece],
            where,
        )

    w_count = [0]

    def w_go(source, target, piece, where, when=None):
        number = w_count[0]
        w_count[0] += 1
        go(w_copy(source, target, piece, number, {"sp": where}), when)

    def w_far(first, past, when=None):
        for piece in range(first, past):
            w_go(y, 2 + y, piece, far, when)

    def w_pass(first, past, when=True):
        for piece in range(first, past):
            pl.when(when)(w_copy(2 + y, 2 + y, piece, 0, {"sp": side}).wait_recv)
            w_go(2 + y, 2 + y, piece, side, when)

    def w_wait(block):
        for piece in range(pieces):
            w_copy(2 * block + 1 - y, 2 * block + 1 - y, piece, 0, {"sp": side}).wait_recv()

    own_a.wait()
    own_b.wait()
    w_far(0, 1)
    w_far(1, pieces - 1, z != 1)
    w_far(pieces - 1, pieces, z > last // 2)
    for piece in range(pieces):
        w_go(y, y, piece, side)

    @pl.when(y == 0)
    def _():
        kv[:, pl.ds(pl.multiple_of(side * rows, rows), rows), :] = jnp.zeros(
            (2, rows, kv.shape[2]), BF16
        )

    diagonal = lax.broadcasted_iota(jnp.int32, (rows, rows), 0) == lax.broadcasted_iota(
        jnp.int32, (rows, rows), 1
    )

    def to_lanes(column):
        return jnp.sum(jnp.where(diagonal, column, 0.0), axis=0, keepdims=True)

    def to_sublanes(row):
        return jnp.sum(jnp.where(diagonal, row, 0.0), axis=1, keepdims=True)

    load_gain.wait()
    gain = gain_v[...].astype(F32)[None, :]

    def norm_rows(slot):
        floats = tok[slot].astype(F32)
        scaled = floats * lax.rsqrt(jnp.mean(floats * floats, axis=-1, keepdims=True) + 1e-06)
        normed[pl.ds(pl.multiple_of(slot * rows_in, rows_in), rows_in), :] = (
            scaled * gain
        ).astype(BF16)

    def tok_wait(slot):
        for part in range(2):
            tok_copy(slot, part, 0, {"tp": core}).wait_recv()

    with scope("norm0"):
        norm_rows(t)
    with scope("tokw1"):
        tok_wait(core)
    with scope("norm1"):
        norm_rows(core)
    with scope("tokw2"):
        for part in range(2):
            tok_copy(cross, part, 0, {"tp": core}).wait_recv()
            go(tok_copy(cross, part, 4 + part, {"tp": core}))
    with scope("norm2"):
        norm_rows(cross)
    with scope("tokw3"):
        tok_wait(diag)
    with scope("norm3"):
        norm_rows(diag)

    def project(weight):
        return jnp.dot(normed[...], weight[...], preferred_element_type=F32)

    own_rows = pl.ds(pl.multiple_of(s * rows, rows), rows)
    kv_count = [0]

    def kv_go(slot, part, where, when):
        piece = kv.at[part, pl.ds(pl.multiple_of(slot * rows, rows), rows)]
        number = kv_count[0]
        kv_count[0] += 1
        go(
            remote(piece, piece, kv_send.at[number], kv_recv.at[slot, part], {"sp": where}),
            when,
        )

    def kv_wait(slot, part, when):
        piece = kv.at[part, pl.ds(pl.multiple_of(slot * rows, rows), rows)]
        copy = remote(piece, piece, kv_send.at[0], kv_recv.at[slot, part], {"sp": side})
        pl.when(when)(copy.wait_recv)

    def kv_pass(distance, part, when):
        slot = rem(s + n_sp - 2 * distance, n_sp)
        kv_wait(slot, part, when)
        if distance < last:
            kv_go(slot, part, up, when & (z == last - 1))
        kv_go(slot, part, side, when)

    with scope("projkv"):
        load_k.wait()
        load_v.wait()
        for part, weight in enumerate((wk, wv)):
            kv[part, own_rows, :] = project(weight).astype(BF16)
            kv_go(s, part, up, z < last)
            kv_go(s, part, up_two, z == 0)
            kv_go(s, part, side, y == 0)
    rim = rim_out.shape[0]
    with scope("glu"):
        load_cv.wait()
        load_cg.wait()
        glu = (project(wcv) * jax.nn.sigmoid(project(wcg))).astype(BF16)
        rim_out[...] = glu[rows - rim :]
    rim_copy = remote(rim_out, rim_in, rim_sem.at[0], rim_sem.at[1], {"sp": after})
    go(rim_copy)
    with scope("projq"):
        pad[pl.ds(rim, rows), :] = glu.astype(F32)
        load_q.wait()
        query = project(wq).astype(BF16)
    w_pass(0, 1, z == last)
    with scope("kvp1"):
        for part in range(2):
            kv_pass(1, part, z >= 1)
        for part in range(2):
            kv_pass(2, part, z == last - 1)
    w_pass(1, 2, z == last)
    with scope("rimw"):
        load_taps.wait()
        rim_copy.wait_recv()
    with scope("conv"):
        pad[pl.ds(0, rim), :] = jnp.where(s == 0, 0.0, rim_in[...].astype(F32))
        lead = rim - (KW - 1)
        conv = jnp.zeros((rows, ccols), F32)
        for tap in range(KW):
            conv = conv + taps[pl.ds(tap, 1), :].astype(F32) * pad[pl.ds(lead + tap, rows), :]
        stat[t] = jnp.zeros(stat.shape[1:], F32)
        stat[t, pl.ds(0, 1), :] = to_lanes(jnp.sum(conv, axis=1, keepdims=True))
        stat[t, pl.ds(1, 1), :] = to_lanes(jnp.sum(conv * conv, axis=1, keepdims=True))

    def stat_copy(slot, number, where):
        return remote(stat.at[slot], stat.at[slot], stat_send.at[number], stat_recv.at[slot], where)

    for number, peer in enumerate((core, cross, diag)):
        go(stat_copy(t, number, {"tp": peer}))
    w_far(1, pieces, z == 1)
    with scope("kvp2"):
        for part in range(2):
            kv_pass(2, part, z == last)
    with scope("wp0"):
        w_pass(0, 1, z < last)
        w_pass(1, pieces, z <= last // 2)
        w_pass(2, pieces - 1, z == last)
    def act_copy(first, size, number):
        span = pl.ds(first, size)
        return remote(
            act.at[0, :, span],
            act.at[1, :, span],
            act_send.at[number],
            act_recv.at[number],
            {"sp": mate},
        )

    act_copies = [act_copy(half, ccols, 0)]
    act_copies += [act_copy(head * HEAD, HEAD, 1 + head) for head in range(head_count)]

    def attend(layer):
        for distance in range(layer + 1):
            for part in range(2):
                slot = rem(side + n_sp - 2 * distance, n_sp)
                kv_wait(slot, part, True if distance else y == 1)
        length = 2 * (layer + 1) * rows
        scale = 1.0 / math.sqrt(HEAD)
        key_places = lax.broadcasted_iota(jnp.int32, (rows, length), 1)
        allowed = key_places <= s * rows + lax.broadcasted_iota(jnp.int32, (rows, length), 0)
        load_gate.wait()
        for head in range(head_count):
            scores = (
                lax.dot_general(
                    query[:, head * HEAD : (head + 1) * HEAD],
                    kv[0, pl.ds(0, length)],
                    (((1,), (1,)), ((), ())),
                    preferred_element_type=F32,
                )
                * scale
            )
            query_gate = to_sublanes(gate[pl.ds(head, 1), own_rows])
            logits = scores + query_gate - gate[pl.ds(head, 1), pl.ds(0, length)]
            logits = jnp.where(allowed, logits, -1e30)
            weights = jnp.exp(logits - jnp.max(logits, axis=-1, keepdims=True))
            denom = jnp.sum(weights, axis=-1, keepdims=True)
            numer = jnp.dot(
                weights.astype(BF16), kv[1, pl.ds(0, length)], preferred_element_type=F32
            )
            act[0, :, pl.ds(head * HEAD, HEAD)] = (numer / denom).astype(BF16)
            act_copies[1 + head].start()

    for layer in range(last):

        @pl.when(z == layer)
        def _():
            with scope("attn_early"):
                attend(layer)

    w_far(pieces - 1, pieces, z == 0)
    with scope("statw"):
        load_cgain.wait()
        load_cbias.wait()
        for peer in (core, cross, diag):
            stat_copy(peer, 0, {"tp": core}).wait_recv()

    with scope("convact"):
        totals = stat[0]
        for peer in range(1, n_tp):
            totals = totals + stat[peer]
        channels = n_tp * ccols
        mean_c = to_sublanes(totals[0:1]) / channels
        var_c = to_sublanes(totals[1:2]) / channels - mean_c * mean_c
        shaped = (conv - mean_c) * lax.rsqrt(var_c + 1e-05) * cgain_v[...].astype(F32)[
            None, :
        ] + cbias_v[...].astype(F32)[None, :]
        act[0, :, pl.ds(half, ccols)] = (shaped / (1.0 + jnp.exp(-shaped))).astype(BF16)
    go(act_copies[0])
    with scope("kvp3"):
        for part in range(2):
            kv_pass(3, part, z == last)
    @pl.when(z == last)
    def _():
        with scope("attn_late"):
            attend(last)

    sent.extend((copy, None) for copy in act_copies[1:])
    with scope("wp1"):
        w_pass(1, pieces, z == last - 1)
        w_pass(pieces - 1, pieces, z == last)
    with scope("wnear"):
        w_wait(0)

    def columns(part):
        return pl.ds(part * wide, wide)

    def product(row_set, block, part):
        return jnp.dot(
            act[row_set], wbuf[2 * block + part], preferred_element_type=F32
        )

    def pair_copy(row_set, part):
        return remote(
            pair_out.at[row_set, :, columns(part)],
            pair_in.at[row_set, :, columns(part)],
            pair_send.at[row_set, part],
            pair_recv.at[row_set, part],
            {"tp": core},
        )

    def ship(row_set, block):
        for part in range(2):
            pair_out[row_set, :, columns(part)] = product(row_set, block, part).astype(BF16)
            pair_copy(row_set, part).start()

    def keep(row_set, block):
        for part in range(2):
            acc[row_set, :, columns(part)] = product(row_set, block, part)

    def sum_copy(source, target, part, where):
        return remote(
            sum_out.at[source, :, columns(part)],
            sum_in.at[target, :, columns(part)],
            sum_send.at[source, part],
            sum_recv.at[target, part],
            where,
        )

    away = jnp.logical_not(home)
    own_sum = [sum_copy(0, 0, part, {"tp": cross}) for part in range(2)]
    mate_home = [sum_copy(1, 1, part, {"sp": mate}) for part in range(2)]
    mate_away = [sum_copy(1, 0, part, {"sp": mate, "tp": cross}) for part in range(2)]

    def finish(row_set):
        for part in range(2):
            pair_copy(row_set, part).wait_recv()
            total = acc[row_set, :, columns(part)] + pair_in[row_set, :, columns(part)].astype(F32)
            if row_set == 0:
                acc[0, :, columns(part)] = total
            sum_out[row_set, :, columns(part)] = total.astype(BF16)
            if row_set == 0:
                pl.when(away)(own_sum[part].start)
            else:
                pl.when(home)(mate_home[part].start)
                pl.when(away)(mate_away[part].start)

    def mate_wait():
        for copy in act_copies:
            copy.wait_recv()

    @pl.when(near_mine)
    def _():
        with scope("a_near0"):
            keep(0, 0)
        with scope("a_mate"):
            mate_wait()
        with scope("a_near1"):
            keep(1, 0)
        with scope("a_fin1"):
            finish(1)
        with scope("a_fin0"):
            finish(0)
        with scope("a_wfar"):
            w_wait(1)
        with scope("a_far"):
            ship(1, 1)
            ship(0, 1)

    @pl.when(jnp.logical_not(near_mine))
    def _():
        with scope("b_near0"):
            ship(0, 0)
        with scope("b_mate"):
            mate_wait()
        with scope("b_near1"):
            ship(1, 0)
        with scope("b_wfar"):
            w_wait(1)
        with scope("b_far"):
            keep(1, 1)
            keep(0, 1)
        with scope("b_fin1"):
            finish(1)
        with scope("b_fin0"):
            finish(0)

    @pl.when(home)
    def _():
        for part in range(2):
            with scope("c_home"):
                own_sum[part].wait_recv()
            span = columns(part)
            out_r[:, span] = (acc[0, :, span] + sum_in[0, :, span].astype(F32)).astype(BF16)

    @pl.when(away)
    def _():
        for part in range(2):
            with scope("c_away"):
                mate_home[part].wait_recv()
                mate_away[part].wait_recv()
            span = columns(part)
            out_r[:, span] = (
                sum_in[0, :, span].astype(F32) + sum_in[1, :, span].astype(F32)
            ).astype(BF16)

    for part in range(2):
        sent.extend((pair_copy(row_set, part), None) for row_set in range(2))
        sent.append((own_sum[part], away))
        sent.append((mate_home[part], None))
    with scope("sendw"):
        for copy, when in sent:
            if when is None:
                copy.wait_send()
            else:
                pl.when(when)(copy.wait_send)


def fused(n_sp, n_tp, *args):
    tokens, gain, wq, wk, wv, wcv, wcg, taps, cgain, cbias, gate, woa, woc = args
    rows_in, width = tokens.shape
    rows = rows_in * n_tp
    rim = -(-(KW - 1) // 16) * 16
    wide = woa.shape[1]
    out_wide = wide * n_sp // n_tp
    both = woa.shape[0] + woc.shape[0]
    pieces = 4
    heads = gate.shape[1]
    hbm = pl.BlockSpec(memory_space=pltpu.HBM)
    vmem = pl.BlockSpec(memory_space=pltpu.VMEM)
    dma = pltpu.SemaphoreType.DMA
    scratch = [
        pltpu.VMEM((n_tp, rows_in, width), BF16),
        pltpu.VMEM((rows, width), BF16),
        *[pltpu.VMEM(w.shape, w.dtype) for w in (wq, wk, wv, wcv, wcg, taps)],
        pltpu.VMEM(gate.shape[::-1], F32),
        pltpu.VMEM(gain.shape, BF16),
        pltpu.VMEM(cgain.shape, BF16),
        pltpu.VMEM(cbias.shape, BF16),
        pltpu.VMEM((4, both, wide), BF16),
        pltpu.VMEM((2, n_sp * rows, wk.shape[1]), BF16),
        pltpu.VMEM((rim + rows, wcv.shape[1]), F32),
        pltpu.VMEM((rim, wcv.shape[1]), BF16),
        pltpu.VMEM((rim, wcv.shape[1]), BF16),
        pltpu.VMEM((n_tp, 8, rows), F32),
        pltpu.VMEM((2, rows, both), BF16),
        pltpu.VMEM((2, rows, out_wide), F32),
        *[pltpu.VMEM((2, rows, out_wide), BF16)] * 4,
        dma((13,)),
        dma((6,)),
        dma((n_tp, 2)),
        dma((12 * pieces,)),
        dma((4, pieces)),
        dma((32,)),
        dma((n_sp, 2)),
        dma((2,)),
        dma((3,)),
        dma((n_tp,)),
        dma((1 + heads,)),
        dma((1 + heads,)),
        *[dma((2, 2))] * 4,
    ]
    result = pltpu.VMEM((rows, out_wide), BF16)
    spare = 3 * rows * out_wide
    return pl.pallas_call(
        functools.partial(fused_kernel, n_sp, n_tp),
        out_shape=result,
        in_specs=[hbm] * 13,
        out_specs=vmem,
        scratch_shapes=scratch,
        compiler_params=pltpu.CompilerParams(
            collective_id=0, has_side_effects=True, vmem_limit_bytes=67_043_328 - spare
        ),
    )(
        tokens, gain, wq, wk, wv, wcv, wcg, taps,
        cgain, cbias, gate.T, woa, woc,
    )


def layer(sizes, *args):
    n_sp, n_tp = sizes["sp"], sizes["tp"]
    tokens, wq, wk, wcv, woa, woc = (args[k] for k in (0, 2, 3, 5, 11, 12))
    fits = (
        n_sp == 8
        and n_tp == 4
        and tokens.shape[0] * n_tp == HEAD
        and wk.shape[1] == HEAD
        and woa.shape[1] % HEAD == 0
        and woa.shape == woc.shape
        and wq.shape[1] == wcv.shape[1] == woa.shape[0]
    )
    if fits:
        return fused(n_sp, n_tp, *args)
    return shards(*args)


def solution(mesh):
    return jax.shard_map(
        functools.partial(layer, dict(mesh.shape)),
        mesh=mesh,
        in_specs=(
            P(("sp", "tp"), None),
            P(),
            P(None, "tp"),
            P(None, "tp"),
            P(None, "tp"),
            P(None, "tp"),
            P(None, "tp"),
            P(None, "tp"),
            P("tp"),
            P("tp"),
            P(None, "tp"),
            P("tp", "sp"),
            P("tp", "sp"),
        ),
        out_specs=P("sp", "tp"),
        check_vma=False,
    )
```

time: 42.6 us -> 33.6 us (0.79)
  the two profiles are of different devices: /device:TPU:24 before, /device:TPU:17 now
where the time goes in v2:
time: 33.6 us; the launch traced here: 33.4 us
  Pallas kernels  32.8 us (98%)
  local copies, waits for them, and re-layouts  0.66 us (2%)
    pallas_call x1, Pallas kernels, fused(): pl.pallas_call(functools.partial(fused_kernel, n_sp, n_tp), out_shape=res...  32.8 us

profile of v2, /device:TPU:17, one launch (start us, length us, event | category | flops | bytes accessed | tf_op | source)
XLA Modules:
  0.0 33.4 jit_solution(9628527821338217950)
XLA Ops:
  0.0 32.8 %shard_map.127 = bf16[128,512]{1,0:T(8,128)(2,1)S(1)} custom-call(bf16[32,2048]{1,0:T(8,128)(2,1)} %tokens_h.1, bf16[2048]{0:T(1024)(128)(2,1)} %gain_h.1, bf16[2048,256]{1,0:T(8,128)(2,1)} %wq_h.1, bf16[2048,128]{1,0:T(8,128)(2,1)} %wk_h.1, bf16[2048,128]{1,0:T(8,128)(2,1)} %wv_h.1, bf16[2048,256]{1,0:T(8,128)(2,1)} %wcv_h.1, bf16[2048,256]{1,0:T(8,128)(2,1)} %wcg_h.1, ...), custom_call_target="tpu_custom_call" | custom-call | tf_op jit(solution)/shard_map/pallas_call | solution.py:725
  32.8 0.7 %copy.15 = bf16[128,512]{1,0:T(8,128)(2,1)} copy(bf16[128,512]{1,0:T(8,128)(2,1)S(1)} %shard_map.127) | data formatting | bytes 262144

commit v3 on v2

--- a/solution.py
+++ b/solution.py
@@ -155,6 +155,12 @@
 F32 = jnp.float32
 BF16 = jnp.bfloat16
 
+AT_ONCE = 1
+SPLIT_FROM = 2
+FAR = ((0, 1, 1, 5), (0, 2, 3, 3), (0, 0, 0, 0), (0, 0, 0, 0))
+NEAR = (0, 0, 0, 0)
+PASS = ((2, 2, 3, 3), (2, 3, 4, 4), (2, 4, 6, 6), (2, 3, 6, 7))
+
 
 def fused_kernel(
     n_sp,
@@ -176,8 +182,7 @@
     tok,
     normed,
     wq,
-    wk,
-    wv,
+    wkv,
     wcv,
     wcg,
     taps,
@@ -187,6 +192,7 @@
     cbias_v,
     wbuf,
     kv,
+    query,
     pad,
     rim_out,
     rim_in,
@@ -262,8 +268,9 @@
     own_b = local(woc_h, wbuf.at[y, pl.ds(half, half)], 2)
     load_gate = local(gate_h, gate, 3)
     load_gain = local(gain_h, gain_v, 10)
-    load_k = local(wk_h, wk, 4)
-    load_v = local(wv_h, wv, 5)
+    kv_cols = wk_h.shape[1]
+    load_k = local(wk_h, wkv.at[:, pl.ds(0, kv_cols)], 4)
+    load_v = local(wv_h, wkv.at[:, pl.ds(kv_cols, kv_cols)], 5)
     load_cv = local(wcv_h, wcv, 6)
     load_cg = local(wcg_h, wcg, 7)
     load_q = local(wq_h, wq, 8)
@@ -298,9 +305,9 @@
         return remote(piece, piece, tok_send.at[number], tok_recv.at[slot, part], where)
 
     for part in range(2):
+        go(tok_copy(t, part, 2 + part, {"tp": core}))
+    for part in range(2):
         go(tok_copy(t, part, part, {"tp": cross}))
-    for part in range(2):
-        go(tok_copy(t, part, 2 + part, {"tp": core}))
 
     def w_copy(source, target, piece, number, where):
         span = pl.ds(piece * deep, deep)
@@ -312,21 +319,21 @@
             where,
         )
 
-    w_count = [0]
-
-    def w_go(source, target, piece, where, when=None):
-        number = w_count[0]
-        w_count[0] += 1
-        go(w_copy(source, target, piece, number, {"sp": where}), when)
-
-    def w_far(first, past, when=None):
-        for piece in range(first, past):
-            w_go(y, 2 + y, piece, far, when)
-
-    def w_pass(first, past, when=True):
-        for piece in range(first, past):
-            pl.when(when)(w_copy(2 + y, 2 + y, piece, 0, {"sp": side}).wait_recv)
-            w_go(2 + y, 2 + y, piece, side, when)
+    far_copies = [w_copy(y, 2 + y, piece, piece, {"sp": far}) for piece in range(pieces)]
+    pass_copies = [
+        w_copy(2 + y, 2 + y, piece, 2 * pieces + piece, {"sp": side}) for piece in range(pieces)
+    ]
+
+    def pass_on(layer, point):
+        for copy, turn in zip(pass_copies, PASS[layer]):
+            if turn == point:
+                copy.wait_recv()
+                copy.start()
+
+    def w_pass(point):
+        for layer in range(last + 1):
+            if point in PASS[layer]:
+                pl.when(z == layer)(functools.partial(pass_on, layer, point))
 
     def w_wait(block):
         for piece in range(pieces):
@@ -334,11 +341,15 @@
 
     own_a.wait()
     own_b.wait()
-    w_far(0, 1)
-    w_far(1, pieces - 1, z != 1)
-    w_far(pieces - 1, pieces, z > last // 2)
-    for piece in range(pieces):
-        w_go(y, y, piece, side)
+    def release(point):
+        for piece in range(pieces):
+            for layer in range(last + 1):
+                if FAR[layer][piece] == point:
+                    pl.when(z == layer)(far_copies[piece].start)
+            if NEAR[piece] == point:
+                go(w_copy(y, y, piece, pieces + piece, {"sp": side}))
+
+    release(0)
 
     @pl.when(y == 0)
     def _():
@@ -370,12 +381,70 @@
         for part in range(2):
             tok_copy(slot, part, 0, {"tp": core}).wait_recv()
 
+    mid = rows // 2
+    starts = [rem(t // 2 + part, 2) * mid for part in range(2)]
+
+    def half_rows(part, offset=0):
+        return pl.ds(pl.multiple_of(offset + starts[part], mid), mid)
+
+    def project(weight, part):
+        return jnp.dot(normed[half_rows(part), :], weight[...], preferred_element_type=F32)
+
+    own_rows = pl.ds(pl.multiple_of(s * rows, rows), rows)
+
+    def kv_copy(slot, part, number, where):
+        piece = kv.at[:, half_rows(part, slot * rows)]
+        return remote(piece, piece, kv_send.at[number], kv_recv.at[slot, part], {"sp": where})
+
+    def kv_wait(slot, part, when):
+        pl.when(when)(kv_copy(slot, part, 0, side).wait_recv)
+
+    def kv_pass(distance, part, when):
+        slot = rem(s + n_sp - 2 * distance, n_sp)
+        number = 2 + 4 * distance + 2 * part
+        kv_wait(slot, part, when)
+        if distance < last:
+            go(kv_copy(slot, part, number, up), when & (z == last - 1))
+        go(kv_copy(slot, part, number + 1, side), when)
+
+    def kv_own(part):
+        both = project(wkv, part).astype(BF16)
+        for column in range(2):
+            kv[column, half_rows(part, s * rows), :] = both[
+                :, column * kv_cols : (column + 1) * kv_cols
+            ]
+        go(kv_copy(s, part, 3 * part + 1, up_two), z == 0)
+        go(kv_copy(s, part, 3 * part, up), z < last)
+        go(kv_copy(s, part, 3 * part + 2, side), y == 0)
+
+    rim = rim_out.shape[0]
+
+    def glu_own(part):
+        glu = project(wcv, part) * jax.nn.sigmoid(project(wcg, part))
+        span = pl.ds(pl.multiple_of(rim + starts[part], rim), mid)
+        pad[span, :] = glu.astype(BF16).astype(F32)
+
+    def query_own(part):
+        query[half_rows(part), :] = project(wq, part).astype(BF16)
+
     with scope("norm0"):
         norm_rows(t)
     with scope("tokw1"):
         tok_wait(core)
     with scope("norm1"):
         norm_rows(core)
+    with scope("kv0"):
+        load_k.wait()
+        load_v.wait()
+        kv_own(0)
+    release(1)
+    with scope("glu0"):
+        load_cv.wait()
+        load_cg.wait()
+        glu_own(0)
+    with scope("q0"):
+        load_q.wait()
+        query_own(0)
     with scope("tokw2"):
         for part in range(2):
             tok_copy(cross, part, 0, {"tp": core}).wait_recv()
@@ -386,61 +455,24 @@
         tok_wait(diag)
     with scope("norm3"):
         norm_rows(diag)
-
-    def project(weight):
-        return jnp.dot(normed[...], weight[...], preferred_element_type=F32)
-
-    own_rows = pl.ds(pl.multiple_of(s * rows, rows), rows)
-    kv_count = [0]
-
-    def kv_go(slot, part, where, when):
-        piece = kv.at[part, pl.ds(pl.multiple_of(slot * rows, rows), rows)]
-        number = kv_count[0]
-        kv_count[0] += 1
-        go(
-            remote(piece, piece, kv_send.at[number], kv_recv.at[slot, part], {"sp": where}),
-            when,
-        )
-
-    def kv_wait(slot, part, when):
-        piece = kv.at[part, pl.ds(pl.multiple_of(slot * rows, rows), rows)]
-        copy = remote(piece, piece, kv_send.at[0], kv_recv.at[slot, part], {"sp": side})
-        pl.when(when)(copy.wait_recv)
-
-    def kv_pass(distance, part, when):
-        slot = rem(s + n_sp - 2 * distance, n_sp)
-        kv_wait(slot, part, when)
-        if distance < last:
-            kv_go(slot, part, up, when & (z == last - 1))
-        kv_go(slot, part, side, when)
-
-    with scope("projkv"):
-        load_k.wait()
-        load_v.wait()
-        for part, weight in enumerate((wk, wv)):
-            kv[part, own_rows, :] = project(weight).astype(BF16)
-            kv_go(s, part, up, z < last)
-            kv_go(s, part, up_two, z == 0)
-            kv_go(s, part, side, y == 0)
-    rim = rim_out.shape[0]
-    with scope("glu"):
-        load_cv.wait()
-        load_cg.wait()
-        glu = (project(wcv) * jax.nn.sigmoid(project(wcg))).astype(BF16)
-        rim_out[...] = glu[rows - rim :]
+    with scope("kv1"):
+        kv_own(1)
+    with scope("glu1"):
+        glu_own(1)
+        rim_out[...] = pad[pl.ds(rows, rim), :].astype(BF16)
     rim_copy = remote(rim_out, rim_in, rim_sem.at[0], rim_sem.at[1], {"sp": after})
     go(rim_copy)
-    with scope("projq"):
-        pad[pl.ds(rim, rows), :] = glu.astype(F32)
-        load_q.wait()
-        query = project(wq).astype(BF16)
-    w_pass(0, 1, z == last)
+    with scope("q1"):
+        query_own(1)
+    release(2)
+    w_pass(2)
     with scope("kvp1"):
         for part in range(2):
             kv_pass(1, part, z >= 1)
         for part in range(2):
             kv_pass(2, part, z == last - 1)
-    w_pass(1, 2, z == last)
+    release(3)
+    w_pass(3)
     with scope("rimw"):
         load_taps.wait()
         rim_copy.wait_recv()
@@ -459,14 +491,14 @@
 
     for number, peer in enumerate((core, cross, diag)):
         go(stat_copy(t, number, {"tp": peer}))
-    w_far(1, pieces, z == 1)
+    release(4)
     with scope("kvp2"):
         for part in range(2):
             kv_pass(2, part, z == last)
+        for part in range(2):
+            kv_pass(3, part, z == last)
     with scope("wp0"):
-        w_pass(0, 1, z < last)
-        w_pass(1, pieces, z <= last // 2)
-        w_pass(2, pieces - 1, z == last)
+        w_pass(4)
     def act_copy(first, size, number):
         span = pl.ds(first, size)
         return remote(
@@ -480,45 +512,78 @@
     act_copies = [act_copy(half, ccols, 0)]
     act_copies += [act_copy(head * HEAD, HEAD, 1 + head) for head in range(head_count)]
 
+    scale = 1.0 / math.sqrt(HEAD)
+
+    def fold(first, past, states):
+        span = pl.ds(first, past - first)
+        spots = (rows, past - first)
+        key_places = first + lax.broadcasted_iota(jnp.int32, spots, 1)
+        allowed = key_places <= s * rows + lax.broadcasted_iota(jnp.int32, spots, 0)
+        asked = jnp.concatenate(
+            [query[:, head * HEAD : (head + 1) * HEAD] for head in range(head_count)], axis=0
+        )
+        scores = lax.dot_general(
+            asked, kv[0, span], (((1,), (1,)), ((), ())), preferred_element_type=F32
+        )
+        tops, denoms, parts = [], [], []
+        for head in range(head_count):
+            query_gate = to_sublanes(gate[pl.ds(head, 1), own_rows])
+            logits = (
+                scores[head * rows : (head + 1) * rows] * scale
+                + query_gate
+                - gate[pl.ds(head, 1), span]
+            )
+            logits = jnp.where(allowed, logits, -1e30)
+            top = jnp.max(logits, axis=-1, keepdims=True)
+            if states is not None:
+                top = jnp.maximum(top, states[head][0])
+            weights = jnp.exp(logits - top)
+            tops.append(top)
+            denoms.append(jnp.sum(weights, axis=-1, keepdims=True))
+            parts.append(weights.astype(BF16))
+        product = jnp.dot(
+            jnp.concatenate(parts, axis=0), kv[1, span], preferred_element_type=F32
+        )
+        result = []
+        for head in range(head_count):
+            denom, numer = denoms[head], product[head * rows : (head + 1) * rows]
+            if states is not None:
+                factor = jnp.exp(states[head][0] - tops[head])
+                denom = denom + states[head][1] * factor
+                numer = numer + states[head][2] * factor
+            result.append((tops[head], denom, numer))
+        return result
+
     def attend(layer):
-        for distance in range(layer + 1):
+        def arrive(distance):
             for part in range(2):
                 slot = rem(side + n_sp - 2 * distance, n_sp)
                 kv_wait(slot, part, True if distance else y == 1)
-        length = 2 * (layer + 1) * rows
-        scale = 1.0 / math.sqrt(HEAD)
-        key_places = lax.broadcasted_iota(jnp.int32, (rows, length), 1)
-        allowed = key_places <= s * rows + lax.broadcasted_iota(jnp.int32, (rows, length), 0)
+
+        block = 2 * rows
+        split = layer >= SPLIT_FROM
+        for distance in range(layer + 1 - split):
+            arrive(distance)
         load_gate.wait()
+        states = fold(block * split, (layer + 1) * block, None)
+        with scope("wpx"):
+            pass_on(layer, 6)
+        if split:
+            arrive(layer)
+            states = fold(0, block, states)
         for head in range(head_count):
-            scores = (
-                lax.dot_general(
-                    query[:, head * HEAD : (head + 1) * HEAD],
-                    kv[0, pl.ds(0, length)],
-                    (((1,), (1,)), ((), ())),
-                    preferred_element_type=F32,
-                )
-                * scale
-            )
-            query_gate = to_sublanes(gate[pl.ds(head, 1), own_rows])
-            logits = scores + query_gate - gate[pl.ds(head, 1), pl.ds(0, length)]
-            logits = jnp.where(allowed, logits, -1e30)
-            weights = jnp.exp(logits - jnp.max(logits, axis=-1, keepdims=True))
-            denom = jnp.sum(weights, axis=-1, keepdims=True)
-            numer = jnp.dot(
-                weights.astype(BF16), kv[1, pl.ds(0, length)], preferred_element_type=F32
-            )
+            unused, denom, numer = states[head]
             act[0, :, pl.ds(head * HEAD, HEAD)] = (numer / denom).astype(BF16)
             act_copies[1 + head].start()
 
-    for layer in range(last):
+    for layer in range(AT_ONCE):
 
         @pl.when(z == layer)
         def _():
             with scope("attn_early"):
                 attend(layer)
 
-    w_far(pieces - 1, pieces, z == 0)
+    release(5)
     with scope("statw"):
         load_cgain.wait()
         load_cbias.wait()
@@ -537,18 +602,16 @@
         ] + cbias_v[...].astype(F32)[None, :]
         act[0, :, pl.ds(half, ccols)] = (shaped / (1.0 + jnp.exp(-shaped))).astype(BF16)
     go(act_copies[0])
-    with scope("kvp3"):
-        for part in range(2):
-            kv_pass(3, part, z == last)
-    @pl.when(z == last)
-    def _():
-        with scope("attn_late"):
-            attend(last)
-
-    sent.extend((copy, None) for copy in act_copies[1:])
+    for layer in range(AT_ONCE, last + 1):
+
+        @pl.when(z == layer)
+        def _():
+            with scope("attn_late"):
+                attend(layer)
+
+    sent.extend((copy, None) for copy in act_copies[1:] + far_copies + pass_copies)
     with scope("wp1"):
-        w_pass(1, pieces, z == last - 1)
-        w_pass(pieces - 1, pieces, z == last)
+        w_pass(7)
     with scope("wnear"):
         w_wait(0)
 
@@ -609,41 +672,46 @@
         for copy in act_copies:
             copy.wait_recv()
 
-    @pl.when(near_mine)
-    def _():
+    def sums(mine, odd):
         with scope("a_near0"):
-            keep(0, 0)
-        with scope("a_mate"):
-            mate_wait()
-        with scope("a_near1"):
-            keep(1, 0)
-        with scope("a_fin1"):
-            finish(1)
-        with scope("a_fin0"):
-            finish(0)
+            if odd:
+                mate_wait()
+            for row_set in (1, 0) if odd else (0,):
+                (keep if mine else ship)(row_set, 0)
         with scope("a_wfar"):
             w_wait(1)
-        with scope("a_far"):
-            ship(1, 1)
-            ship(0, 1)
-
-    @pl.when(jnp.logical_not(near_mine))
-    def _():
-        with scope("b_near0"):
-            ship(0, 0)
-        with scope("b_mate"):
-            mate_wait()
-        with scope("b_near1"):
-            ship(1, 0)
-        with scope("b_wfar"):
-            w_wait(1)
-        with scope("b_far"):
-            keep(1, 1)
-            keep(0, 1)
-        with scope("b_fin1"):
-            finish(1)
-        with scope("b_fin0"):
-            finish(0)
+        distant = ship if mine else keep
+        if odd:
+            with scope("a_mate"):
+                distant(1, 1)
+            if mine:
+                distant(0, 1)
+            with scope("a_fin1"):
+                finish(1)
+            if not mine:
+                distant(0, 1)
+            with scope("a_fin0"):
+                finish(0)
+        else:
+            distant(0, 1)
+            with scope("a_fin0"):
+                finish(0)
+            with scope("a_mate"):
+                mate_wait()
+            if mine:
+                ship(1, 1)
+                keep(1, 0)
+            else:
+                ship(1, 0)
+                keep(1, 1)
+            with scope("a_fin1"):
+                finish(1)
+
+    for odd in range(2):
+        for mine in range(2):
+            pl.when((rem(z, 2) == odd) & (near_mine if mine else jnp.logical_not(near_mine)))(
+                functools.partial(sums, mine, odd)
+            )
 
     @pl.when(home)
     def _():
@@ -692,13 +760,16 @@
     scratch = [
         pltpu.VMEM((n_tp, rows_in, width), BF16),
         pltpu.VMEM((rows, width), BF16),
-        *[pltpu.VMEM(w.shape, w.dtype) for w in (wq, wk, wv, wcv, wcg, taps)],
+        pltpu.VMEM(wq.shape, BF16),
+        pltpu.VMEM((width, wk.shape[1] + wv.shape[1]), BF16),
+        *[pltpu.VMEM(w.shape, BF16) for w in (wcv, wcg, taps)],
         pltpu.VMEM(gate.shape[::-1], F32),
         pltpu.VMEM(gain.shape, BF16),
         pltpu.VMEM(cgain.shape, BF16),
         pltpu.VMEM(cbias.shape, BF16),
         pltpu.VMEM((4, both, wide), BF16),
         pltpu.VMEM((2, n_sp * rows, wk.shape[1]), BF16),
+        pltpu.VMEM((rows, wq.shape[1]), BF16),
         pltpu.VMEM((rim + rows, wcv.shape[1]), F32),
         pltpu.VMEM((rim, wcv.shape[1]), BF16),
         pltpu.VMEM((rim, wcv.shape[1]), BF16),
@@ -709,9 +780,9 @@
         dma((13,)),
         dma((6,)),
         dma((n_tp, 2)),
-        dma((12 * pieces,)),
+        dma((3 * pieces,)),
         dma((4, pieces)),
-        dma((32,)),
+        dma((18,)),
         dma((n_sp, 2)),
         dma((2,)),
         dma((3,)),

time: 33.6 us -> 31.9 us (0.949)
  the two profiles are of different devices: /device:TPU:17 before, /device:TPU:24 now
where the time goes in v3:
time: 31.9 us; the launch traced here: 31.6 us
  Pallas kernels  30.9 us (97%)
  local copies, waits for them, and re-layouts  0.66 us (2%)
    pallas_call x1, Pallas kernels, fused(): pl.pallas_call(functools.partial(fused_kernel, n_sp, n_tp), out_shape=res...  30.9 us
    unnamed x1, local copies, waits for them, and re-layouts  0.66 us

profile of v3, /device:TPU:24, one launch (start us, length us, event | category | flops | bytes accessed | tf_op | source)
XLA Modules:
  0.0 31.6 jit_solution(3930141204932944229)
XLA Ops:
  0.0 30.9 %shard_map.127 = bf16[128,512]{1,0:T(8,128)(2,1)S(1)} custom-call(bf16[32,2048]{1,0:T(8,128)(2,1)} %tokens_h.1, bf16[2048]{0:T(1024)(128)(2,1)} %gain_h.1, bf16[2048,256]{1,0:T(8,128)(2,1)} %wq_h.1, bf16[2048,128]{1,0:T(8,128)(2,1)} %wk_h.1, bf16[2048,128]{1,0:T(8,128)(2,1)} %wv_h.1, bf16[2048,256]{1,0:T(8,128)(2,1)} %wcv_h.1, bf16[2048,256]{1,0:T(8,128)(2,1)} %wcg_h.1, ...), custom_call_target="tpu_custom_call" | custom-call | tf_op jit(solution)/shard_map/pallas_call | solution.py:796
  30.9 0.7 %copy.15 = bf16[128,512]{1,0:T(8,128)(2,1)} copy(bf16[128,512]{1,0:T(8,128)(2,1)S(1)} %shard_map.127) | data formatting | bytes 262144

commit v4 on v3

--- a/solution.py
+++ b/solution.py
@@ -157,7 +157,7 @@
 
 AT_ONCE = 1
 SPLIT_FROM = 2
-FAR = ((0, 1, 1, 5), (0, 2, 3, 3), (0, 0, 0, 0), (0, 0, 0, 0))
+FAR = ((0, 1, 2, 5), (0, 2, 3, 3), (0, 0, 0, 0), (0, 0, 0, 0))
 NEAR = (0, 0, 0, 0)
 PASS = ((2, 2, 3, 3), (2, 3, 4, 4), (2, 4, 6, 6), (2, 3, 6, 7))
 
@@ -245,7 +245,7 @@
     ccols = wcv_h.shape[1]
     half = woa_h.shape[0]
     wide = wbuf.shape[2]
-    pieces = w_recv.shape[1]
+    pieces = w_recv.shape[0] - 2
     deep = wbuf.shape[1] // pieces
 
     def local(src, dst, index):
@@ -264,19 +264,19 @@
         )
 
     own_tok = local(tokens_h, tok.at[t], 0)
-    own_a = local(woa_h, wbuf.at[y, pl.ds(0, half)], 1)
-    own_b = local(woc_h, wbuf.at[y, pl.ds(half, half)], 2)
+    local(woa_h, wbuf.at[y, pl.ds(0, half)], 1)
+    local(woc_h, wbuf.at[y, pl.ds(half, half)], 1)
     load_gate = local(gate_h, gate, 3)
-    load_gain = local(gain_h, gain_v, 10)
+    load_gain = local(gain_h, gain_v, 2)
     kv_cols = wk_h.shape[1]
-    load_k = local(wk_h, wkv.at[:, pl.ds(0, kv_cols)], 4)
-    load_v = local(wv_h, wkv.at[:, pl.ds(kv_cols, kv_cols)], 5)
+    local(wk_h, wkv.at[:, pl.ds(0, kv_cols)], 4)
+    local(wv_h, wkv.at[:, pl.ds(kv_cols, kv_cols)], 4)
     load_cv = local(wcv_h, wcv, 6)
     load_cg = local(wcg_h, wcg, 7)
     load_q = local(wq_h, wq, 8)
-    load_taps = local(taps_h, taps, 9)
-    load_cgain = local(cgain_h, cgain_v, 11)
-    load_cbias = local(cbias_h, cbias_v, 12)
+    load_taps = local(taps_h, taps, 5)
+    load_cgain = local(cgain_h, cgain_v, 9)
+    load_cbias = local(cbias_h, cbias_v, 10)
 
     with scope("barrier"):
         barrier = pltpu.get_barrier_semaphore()
@@ -300,35 +300,42 @@
 
     tok_half = rows_in // 2
 
-    def tok_copy(slot, part, number, where):
+    def all_sent(ref, sem, when=None):
+        sent.append((remote(ref, ref, sem, sem, {"tp": core}), when))
+
+    def tok_copy(slot, part, sends, lands, where):
         piece = tok.at[slot, pl.ds(part * tok_half, tok_half)]
-        return remote(piece, piece, tok_send.at[number], tok_recv.at[slot, part], where)
+        return remote(piece, piece, tok_send.at[sends], tok_recv.at[lands], where)
 
     for part in range(2):
-        go(tok_copy(t, part, 2 + part, {"tp": core}))
+        tok_copy(t, part, 0, 0, {"tp": core}).start()
     for part in range(2):
-        go(tok_copy(t, part, part, {"tp": cross}))
-
-    def w_copy(source, target, piece, number, where):
+        tok_copy(t, part, 1, 1 + part, {"tp": cross}).start()
+    for group, slot in enumerate((t, t, cross)):
+        all_sent(tok.at[slot], tok_send.at[group])
+
+    def w_copy(source, target, piece, sends, lands, where):
         span = pl.ds(piece * deep, deep)
         return remote(
             wbuf.at[source, span],
             wbuf.at[target, span],
-            w_send.at[number],
-            w_recv.at[target, piece],
+            w_send.at[sends],
+            w_recv.at[lands],
             where,
         )
 
-    far_copies = [w_copy(y, 2 + y, piece, piece, {"sp": far}) for piece in range(pieces)]
-    pass_copies = [
-        w_copy(2 + y, 2 + y, piece, 2 * pieces + piece, {"sp": side}) for piece in range(pieces)
+    far_copies = [
+        w_copy(y, 2 + y, piece, 0, 2 + piece, {"sp": far}) for piece in range(pieces)
     ]
+    pass_copies = [w_copy(2 + y, 2 + y, piece, 2, 1, {"sp": side}) for piece in range(pieces)]
+    for group, slot in enumerate((y, y, 2 + y)):
+        all_sent(wbuf.at[slot], w_send.at[group])
 
     def pass_on(layer, point):
-        for copy, turn in zip(pass_copies, PASS[layer]):
+        for piece, turn in enumerate(PASS[layer]):
             if turn == point:
-                copy.wait_recv()
-                copy.start()
+                far_copies[piece].wait_recv()
+                pass_copies[piece].start()
 
     def w_pass(point):
         for layer in range(last + 1):
@@ -336,18 +343,17 @@
                 pl.when(z == layer)(functools.partial(pass_on, layer, point))
 
     def w_wait(block):
-        for piece in range(pieces):
-            w_copy(2 * block + 1 - y, 2 * block + 1 - y, piece, 0, {"sp": side}).wait_recv()
-
-    own_a.wait()
-    own_b.wait()
+        ref = wbuf.at[2 * block + 1 - y]
+        remote(ref, ref, w_send.at[0], w_recv.at[block], {"sp": side}).wait_recv()
+
+    pltpu.make_async_copy(wbuf.at[y], wbuf.at[y], local_sem.at[1]).wait()
     def release(point):
         for piece in range(pieces):
             for layer in range(last + 1):
                 if FAR[layer][piece] == point:
                     pl.when(z == layer)(far_copies[piece].start)
             if NEAR[piece] == point:
-                go(w_copy(y, y, piece, pieces + piece, {"sp": side}))
+                w_copy(y, y, piece, 1, 0, {"sp": side}).start()
 
     release(0)
 
@@ -377,9 +383,9 @@
             scaled * gain
         ).astype(BF16)
 
-    def tok_wait(slot):
-        for part in range(2):
-            tok_copy(slot, part, 0, {"tp": core}).wait_recv()
+    def tok_wait(slot, lands):
+        ref = tok.at[slot]
+        remote(ref, ref, tok_send.at[0], tok_recv.at[lands], {"tp": core}).wait_recv()
 
     mid = rows // 2
     starts = [rem(t // 2 + part, 2) * mid for part in range(2)]
@@ -392,20 +398,25 @@
 
     own_rows = pl.ds(pl.multiple_of(s * rows, rows), rows)
 
-    def kv_copy(slot, part, number, where):
+    def kv_copy(slot, part, sends, where):
         piece = kv.at[:, half_rows(part, slot * rows)]
-        return remote(piece, piece, kv_send.at[number], kv_recv.at[slot, part], {"sp": where})
-
-    def kv_wait(slot, part, when):
-        pl.when(when)(kv_copy(slot, part, 0, side).wait_recv)
+        lands = n_sp + slot // 2 if where is side else 2 * (slot // 2) + part
+        return remote(piece, piece, kv_send.at[sends], kv_recv.at[lands], {"sp": where})
+
+    def kv_slot(slot):
+        return kv.at[:, pl.ds(pl.multiple_of(slot * rows, rows), rows)]
+
+    def kv_start(slot, part, sends, where, when):
+        pl.when(when)(kv_copy(slot, part, sends, where).start)
+        if part == 1:
+            all_sent(kv_slot(slot), kv_send.at[sends], when)
 
     def kv_pass(distance, part, when):
         slot = rem(s + n_sp - 2 * distance, n_sp)
-        number = 2 + 4 * distance + 2 * part
-        kv_wait(slot, part, when)
+        pl.when(when)(kv_copy(slot, part, 0, up).wait_recv)
         if distance < last:
-            go(kv_copy(slot, part, number, up), when & (z == last - 1))
-        go(kv_copy(slot, part, number + 1, side), when)
+            kv_start(slot, part, 1 + 2 * distance, up, when & (z == last - 1))
+        kv_start(slot, part, 2 + 2 * distance if distance < last else 7, side, when)
 
     def kv_own(part):
         both = project(wkv, part).astype(BF16)
@@ -413,9 +424,9 @@
             kv[column, half_rows(part, s * rows), :] = both[
                 :, column * kv_cols : (column + 1) * kv_cols
             ]
-        go(kv_copy(s, part, 3 * part + 1, up_two), z == 0)
-        go(kv_copy(s, part, 3 * part, up), z < last)
-        go(kv_copy(s, part, 3 * part + 2, side), y == 0)
+        kv_start(s, part, 1, up_two, z == 0)
+        kv_start(s, part, 0, up, z < last)
+        kv_start(s, part, 2, side, y == 0)
 
     rim = rim_out.shape[0]
 
@@ -430,12 +441,11 @@
     with scope("norm0"):
         norm_rows(t)
     with scope("tokw1"):
-        tok_wait(core)
+        tok_wait(core, 0)
     with scope("norm1"):
         norm_rows(core)
     with scope("kv0"):
-        load_k.wait()
-        load_v.wait()
+        pltpu.make_async_copy(wkv, wkv, local_sem.at[4]).wait()
         kv_own(0)
     release(1)
     with scope("glu0"):
@@ -447,12 +457,12 @@
         query_own(0)
     with scope("tokw2"):
         for part in range(2):
-            tok_copy(cross, part, 0, {"tp": core}).wait_recv()
-            go(tok_copy(cross, part, 4 + part, {"tp": core}))
+            tok_copy(cross, part, 1, 1 + part, {"tp": cross}).wait_recv()
+            tok_copy(cross, part, 2, 3, {"tp": core}).start()
     with scope("norm2"):
         norm_rows(cross)
     with scope("tokw3"):
-        tok_wait(diag)
+        tok_wait(diag, 3)
     with scope("norm3"):
         norm_rows(diag)
     with scope("kv1"):
@@ -486,11 +496,12 @@
         stat[t, pl.ds(0, 1), :] = to_lanes(jnp.sum(conv, axis=1, keepdims=True))
         stat[t, pl.ds(1, 1), :] = to_lanes(jnp.sum(conv * conv, axis=1, keepdims=True))
 
-    def stat_copy(slot, number, where):
-        return remote(stat.at[slot], stat.at[slot], stat_send.at[number], stat_recv.at[slot], where)
-
-    for number, peer in enumerate((core, cross, diag)):
-        go(stat_copy(t, number, {"tp": peer}))
+    others = stat.at[pl.ds(0, n_tp - 1)]
+    for peer in (core, cross, diag):
+        remote(
+            stat.at[t], stat.at[t], stat_send.at[0], stat_recv.at[0], {"tp": peer}
+        ).start()
+    all_sent(others, stat_send.at[0])
     release(4)
     with scope("kvp2"):
         for part in range(2):
@@ -499,18 +510,19 @@
             kv_pass(3, part, z == last)
     with scope("wp0"):
         w_pass(4)
-    def act_copy(first, size, number):
+    def act_copy(first, size):
         span = pl.ds(first, size)
         return remote(
             act.at[0, :, span],
             act.at[1, :, span],
-            act_send.at[number],
-            act_recv.at[number],
+            act_send.at[0],
+            act_recv.at[0],
             {"sp": mate},
         )
 
-    act_copies = [act_copy(half, ccols, 0)]
-    act_copies += [act_copy(head * HEAD, HEAD, 1 + head) for head in range(head_count)]
+    act_copies = [act_copy(half, ccols)]
+    act_copies += [act_copy(head * HEAD, HEAD) for head in range(head_count)]
+    whole_act = act_copy(0, half + ccols)
 
     scale = 1.0 / math.sqrt(HEAD)
 
@@ -556,9 +568,12 @@
 
     def attend(layer):
         def arrive(distance):
-            for part in range(2):
-                slot = rem(side + n_sp - 2 * distance, n_sp)
-                kv_wait(slot, part, True if distance else y == 1)
+            slot = rem(side + n_sp - 2 * distance, n_sp)
+            ref = kv_slot(slot)
+            copy = remote(
+                ref, ref, kv_send.at[0], kv_recv.at[n_sp + slot // 2], {"sp": side}
+            )
+            pl.when(True if distance else y == 1)(copy.wait_recv)
 
         block = 2 * rows
         split = layer >= SPLIT_FROM
@@ -587,8 +602,7 @@
     with scope("statw"):
         load_cgain.wait()
         load_cbias.wait()
-        for peer in (core, cross, diag):
-            stat_copy(peer, 0, {"tp": core}).wait_recv()
+        remote(others, others, stat_send.at[0], stat_recv.at[0], {"tp": core}).wait_recv()
 
     with scope("convact"):
         totals = stat[0]
@@ -601,7 +615,7 @@
             None, :
         ] + cbias_v[...].astype(F32)[None, :]
         act[0, :, pl.ds(half, ccols)] = (shaped / (1.0 + jnp.exp(-shaped))).astype(BF16)
-    go(act_copies[0])
+    act_copies[0].start()
     for layer in range(AT_ONCE, last + 1):
 
         @pl.when(z == layer)
@@ -609,7 +623,7 @@
             with scope("attn_late"):
                 attend(layer)
 
-    sent.extend((copy, None) for copy in act_copies[1:] + far_copies + pass_copies)
+    sent.append((whole_act, None))
     with scope("wp1"):
         w_pass(7)
     with scope("wnear"):
@@ -627,7 +641,7 @@
         return remote(
             pair_out.at[row_set, :, columns(part)],
             pair_in.at[row_set, :, columns(part)],
-            pair_send.at[row_set, part],
+            pair_send.at[row_set],
             pair_recv.at[row_set, part],
             {"tp": core},
         )
@@ -645,7 +659,7 @@
         return remote(
             sum_out.at[source, :, columns(part)],
             sum_in.at[target, :, columns(part)],
-            sum_send.at[source, part],
+            sum_send.at[source],
             sum_recv.at[target, part],
             where,
         )
@@ -669,8 +683,7 @@
                 pl.when(away)(mate_away[part].start)
 
     def mate_wait():
-        for copy in act_copies:
-            copy.wait_recv()
+        whole_act.wait_recv()
 
     def sums(mine, odd):
         with scope("a_near0"):
@@ -732,10 +745,10 @@
                 sum_in[0, :, span].astype(F32) + sum_in[1, :, span].astype(F32)
             ).astype(BF16)
 
-    for part in range(2):
-        sent.extend((pair_copy(row_set, part), None) for row_set in range(2))
-        sent.append((own_sum[part], away))
-        sent.append((mate_home[part], None))
+    for row_set in range(2):
+        all_sent(pair_out.at[row_set], pair_send.at[row_set])
+    all_sent(sum_out.at[0], sum_send.at[0], away)
+    all_sent(sum_out.at[1], sum_send.at[1])
     with scope("sendw"):
         for copy, when in sent:
             if when is None:
@@ -753,7 +766,6 @@
     out_wide = wide * n_sp // n_tp
     both = woa.shape[0] + woc.shape[0]
     pieces = 4
-    heads = gate.shape[1]
     hbm = pl.BlockSpec(memory_space=pltpu.HBM)
     vmem = pl.BlockSpec(memory_space=pltpu.VMEM)
     dma = pltpu.SemaphoreType.DMA
@@ -777,19 +789,16 @@
         pltpu.VMEM((2, rows, both), BF16),
         pltpu.VMEM((2, rows, out_wide), F32),
         *[pltpu.VMEM((2, rows, out_wide), BF16)] * 4,
-        dma((13,)),
-        dma((6,)),
-        dma((n_tp, 2)),
-        dma((3 * pieces,)),
-        dma((4, pieces)),
-        dma((18,)),
-        dma((n_sp, 2)),
+        dma((11,)),
+        dma((3,)),
+        dma((4,)),
+        dma((3,)),
+        dma((2 + pieces,)),
+        dma((8,)),
+        dma((n_sp + n_sp // 2,)),
         dma((2,)),
-        dma((3,)),
-        dma((n_tp,)),
-        dma((1 + heads,)),
-        dma((1 + heads,)),
-        *[dma((2, 2))] * 4,
+        *[dma((1,))] * 4,
+        *[dma((2,)), dma((2, 2))] * 2,
     ]
     result = pltpu.VMEM((rows, out_wide), BF16)
     spare = 3 * rows * out_wide

time: 31.9 us -> 30.9 us (0.969)
  Pallas kernels: 30.9 us -> 29.7 us
    pallas_call x1, Pallas kernels: 30.9 us -> 29.7 us  [fused(): pl.pallas_call(functools.partial(fused_kernel, n_sp, n_tp), out_shape=res...]
where the time goes in v4:
time: 30.9 us; the launch traced here: 30.4 us
  Pallas kernels  29.7 us (96%)
  local copies, waits for them, and re-layouts  0.66 us (2%)
    pallas_call x1, Pallas kernels, fused(): pl.pallas_call(functools.partial(fused_kernel, n_sp, n_tp), out_shape=res...  29.7 us
    unnamed x1, local copies, waits for them, and re-layouts  0.66 us

profile of v4, /device:TPU:24, one launch (start us, length us, event | category | flops | bytes accessed | tf_op | source)
XLA Modules:
  0.0 30.4 jit_solution(5807797666971410371)
XLA Ops:
  0.0 29.7 %shard_map.127 = bf16[128,512]{1,0:T(8,128)(2,1)S(1)} custom-call(bf16[32,2048]{1,0:T(8,128)(2,1)} %tokens_h.1, bf16[2048]{0:T(1024)(128)(2,1)} %gain_h.1, bf16[2048,256]{1,0:T(8,128)(2,1)} %wq_h.1, bf16[2048,128]{1,0:T(8,128)(2,1)} %wk_h.1, bf16[2048,128]{1,0:T(8,128)(2,1)} %wv_h.1, bf16[2048,256]{1,0:T(8,128)(2,1)} %wcv_h.1, bf16[2048,256]{1,0:T(8,128)(2,1)} %wcg_h.1, ...), custom_call_target="tpu_custom_call" | custom-call | tf_op jit(solution)/shard_map/pallas_call | solution.py:805
  29.8 0.7 %copy.15 = bf16[128,512]{1,0:T(8,128)(2,1)} copy(bf16[128,512]{1,0:T(8,128)(2,1)S(1)} %shard_map.127) | data formatting | bytes 262144

commit v5 on v4

--- a/solution.py
+++ b/solution.py
@@ -157,9 +157,9 @@
 
 AT_ONCE = 1
 SPLIT_FROM = 2
-FAR = ((0, 1, 2, 5), (0, 2, 3, 3), (0, 0, 0, 0), (0, 0, 0, 0))
-NEAR = (0, 0, 0, 0)
-PASS = ((2, 2, 3, 3), (2, 3, 4, 4), (2, 4, 6, 6), (2, 3, 6, 7))
+FAR = ((0, 0, 1, 1, 2, 2, 5, 5), (0, 0, 2, 2, 3, 3, 3, 3), (0, 0, 0, 0, 0, 0, 0, 0), (0, 0, 0, 0, 0, 0, 0, 0))
+NEAR = (0, 0, 0, 0, 0, 0, 0, 0)
+PASS = ((2, 2, 2, 2, 3, 3, 3, 3), (2, 2, 3, 3, 4, 4, 4, 4), (2, 2, 4, 4, 6, 6, 6, 7), (2, 2, 3, 3, 6, 6, 7, 7))
 
 
 def fused_kernel(
@@ -765,7 +765,7 @@
     wide = woa.shape[1]
     out_wide = wide * n_sp // n_tp
     both = woa.shape[0] + woc.shape[0]
-    pieces = 4
+    pieces = 8
     hbm = pl.BlockSpec(memory_space=pltpu.HBM)
     vmem = pl.BlockSpec(memory_space=pltpu.VMEM)
     dma = pltpu.SemaphoreType.DMA

time: 30.9 us -> 30.8 us (level); the launches traced: 30.4 us -> 30.7 us
  no operation moved by 1% of the time
where the time goes in v5:
time: 30.8 us; the launch traced here: 30.7 us
  Pallas kernels  30 us (97%)
  local copies, waits for them, and re-layouts  0.66 us (2%)
    pallas_call x1, Pallas kernels, fused(): pl.pallas_call(functools.partial(fused_kernel, n_sp, n_tp), out_shape=res...  30 us
    unnamed x1, local copies, waits for them, and re-layouts  0.66 us

profile of v5, /device:TPU:24, one launch (start us, length us, event | category | flops | bytes accessed | tf_op | source)
XLA Modules:
  0.0 30.7 jit_solution(2240749971141531025)
XLA Ops:
  0.0 30.0 %shard_map.127 = bf16[128,512]{1,0:T(8,128)(2,1)S(1)} custom-call(bf16[32,2048]{1,0:T(8,128)(2,1)} %tokens_h.1, bf16[2048]{0:T(1024)(128)(2,1)} %gain_h.1, bf16[2048,256]{1,0:T(8,128)(2,1)} %wq_h.1, bf16[2048,128]{1,0:T(8,128)(2,1)} %wk_h.1, bf16[2048,128]{1,0:T(8,128)(2,1)} %wv_h.1, bf16[2048,256]{1,0:T(8,128)(2,1)} %wcv_h.1, bf16[2048,256]{1,0:T(8,128)(2,1)} %wcg_h.1, ...), custom_call_target="tpu_custom_call" | custom-call | tf_op jit(solution)/shard_map/pallas_call | solution.py:805
  30.0 0.7 %copy.15 = bf16[128,512]{1,0:T(8,128)(2,1)} copy(bf16[128,512]{1,0:T(8,128)(2,1)S(1)} %shard_map.127) | data formatting | bytes 262144
